TPU v7x, 32 devices: a whole 2x2x4 slice. The times are simulated.
32 devices in a mesh: sp: 16 (over z, y, x), tp: 2 (over core).
Axes of the slice: x: 2, y: 2, z: 4, core: 2. Of those that a mesh axis runs over, the one named last changes fastest.
Arguments:
- tokens: bfloat16 [4096, 2048], P('sp', 'tp'), may hold values from -6 to 6
- norm_gain: float32 [2048], replicated, may hold values from 0.1 to 1.9
- glu_value: bfloat16 [2048, 2048], P('sp', 'tp'), may hold values from -0.125 to 0.125
- glu_gate: bfloat16 [2048, 2048], P('sp', 'tp'), may hold values from -0.125 to 0.125
- conv_taps: float32 [31, 2048], P(None, 'tp'), may hold values from -11 to 11
- ln_gain: float32 [2048], P('tp'), may hold values from 0.1 to 1.9
- ln_bias: float32 [2048], P('tp'), may hold values from -3 to 3
- query_weight: bfloat16 [2048, 2048], P('sp', 'tp'), may hold values from -0.125 to 0.125
- key_weight: bfloat16 [2048, 2048], P('sp', 'tp'), may hold values from -0.125 to 0.125
- value_weight: bfloat16 [2048, 2048], P('sp', 'tp'), may hold values from -0.125 to 0.125
- gate_weight: bfloat16 [2048, 32], replicated, may hold values from -0.125 to 0.125
- gate_bias: float32 [32], replicated, may hold values from -1 to 110
- log_decay_extra: float32 [4096, 16], P('sp'), may hold values from -1.3 to 0
- mem_gain: float32 [2048], P('tp'), may hold values from 0.1 to 1.9
- out_conv: bfloat16 [2048, 2048], P('tp'), may hold values from -0.125 to 0.125
- out_mem: bfloat16 [2048, 2048], P('tp'), may hold values from -0.125 to 0.125
Outputs:
- mixed: bfloat16 [4096, 2048], P(('sp', 'tp'))
All inputs are finite; a program needn't handle non-finite values.
Results may differ from a plain program's by a relative error of at most 0.015.
Values may be sent and summed in bfloat16 or wider, within the bound.
No kernel may reach another device: no remote copies, remote signals or barrier semaphores. Data moves between devices by JAX's collectives and lax.ppermute only.
A program may use at most 128 MiB of HBM per device.

v0:
```python
import functools
import jax
import jax.numpy as jnp
from jax import lax
from jax.experimental import pallas as pl
from jax.experimental.pallas import tpu as pltpu
from jax.sharding import PartitionSpec as P


MEMORY_HEADS = 8
HEAD = 256
KW = 31
REACH = KW // 2
HALO = 16
TAIL = 16

EPS = 1e-06
LOW_START = -1e30
RING_MOST = 8
F32 = jnp.float32
BF16 = jnp.bfloat16


def params(**kw):
    return pltpu.CompilerParams(vmem_limit_bytes=24 * 1024 * 1024, **kw)


def whole(shape):
    return pl.BlockSpec(shape, lambda i, tab: (0,) * len(shape))


def dot(a, b):
    return jnp.dot(a, b, preferred_element_type=F32)


def dot_nt(a, b, **kw):
    return lax.dot_general(a, b, (((1,), (1,)), ((), ())), preferred_element_type=F32, **kw)


def dot_tn(a, b):
    return lax.dot_general(a, b, (((0,), (0,)), ((), ())), preferred_element_type=F32)


def scan_lanes(x, op, identity, reverse):
    width = x.shape[1]
    lane = lax.broadcasted_iota(jnp.int32, x.shape, 1)
    step = 1
    while step < width:
        if reverse:
            moved = pltpu.roll(x, width - step, 1)
            keep = lane < width - step
        else:
            moved = pltpu.roll(x, step, 1)
            keep = lane >= step
        x = op(x, jnp.where(keep, moved, identity))
        step *= 2
    return x


def log_sigmoid(x):
    return jnp.minimum(x, 0.0) - jnp.log1p(jnp.exp(-jnp.abs(x)))


def split3(x):
    high = x.astype(BF16)
    rest = x - high.astype(F32)
    mid = rest.astype(BF16)
    low = (rest - mid.astype(F32)).astype(BF16)
    return high.astype(F32), mid.astype(F32), low.astype(F32)


def fetch(copies):
    made = [pltpu.make_async_copy(source, target, sem) for source, target, sem in copies]
    for copy in made:
        copy.start()
    return made


def fetch_parts(tab, group, parts, held, sems):
    count, wide = held.shape[2:]
    copies = []
    for block in range(group):
        rows = pl.ds(pl.multiple_of(tab[2 * group + block] * count, count), count)
        for place, part in enumerate(parts):
            copies.append(
                (part.at[rows, pl.ds(0, wide)], held.at[place, block], sems.at[block * len(parts) + place])
            )
    made = fetch(copies)
    return [made[block * len(parts) : (block + 1) * len(parts)] for block in range(group)]


def fetch_weights(tab, group, blocks, rows, pieces, scratches, sems):
    kinds = len(scratches)
    first = 3 * group + 5
    per = pieces[0].shape[0] // (rows * kinds)
    copies = []
    for block in range(blocks):
        start = pl.multiple_of(tab[first + block], rows)
        for kind, scratch in enumerate(scratches):
            at = (block % per * kinds + kind) * rows
            copies.append(
                (pieces[block // per].at[pl.ds(at, rows), :], scratch.at[pl.ds(start, rows), :], sems.at[kind])
            )
    fetch(copies)
    return [pltpu.make_async_copy(x, x, sems.at[kind]) for kind, x in enumerate(scratches)]


def arrived(copies):
    for copy in copies:
        copy.wait()


def project(held, weights):
    total = None
    for place, part in enumerate(held):
        wide = part.shape[1]
        term = dot(part, weights[place * wide : (place + 1) * wide, :])
        total = term if total is None else total + term
    return total


def gates_kernel(dims, tab, *refs):
    group, n_parts, extra_at, key_scale = dims
    parts = refs[:n_parts]
    extra, gate_rows, gate_bias, rows_out, held, extra_in, rows_in, gates, extras, part_sems, sems = refs[n_parts:]
    core, head = tab[3 * group + 2], tab[3 * group + 4]
    waits = fetch_parts(tab, group, parts, held, part_sems)
    count = held.shape[2]
    copies = [(gate_rows, rows_in, sems.at[group])]
    for block in range(group):
        rows = pl.ds(pl.multiple_of(tab[2 * group + block] * count, count), count)
        copies.append((extra.at[rows, pl.ds(extra_at * 128, 128)], extra_in.at[block], sems.at[block]))
    rows_wait, *extra_waits = fetch(copies)
    line = lax.broadcasted_iota(jnp.int32, (2 * MEMORY_HEADS, 128), 0)
    column = lax.broadcasted_iota(jnp.int32, (2 * MEMORY_HEADS, 128), 1)
    select = (column % (2 * MEMORY_HEADS) == line) & (column < 6 * MEMORY_HEADS)
    select = jnp.where(select, 1.0, 0.0).astype(BF16)
    rows_wait.wait()
    for block in range(group):
        here = slice(block * count, (block + 1) * count)
        arrived(waits[block])
        pre = None
        for place in range(n_parts):
            wide = held.shape[3]
            start = 0 if n_parts == 1 else pl.multiple_of((core if place == 0 else 1 - core) * wide, wide)
            term = dot_nt(rows_in[:, pl.ds(start, wide)], held[place, block])
            pre = term if pre is None else pre + term
        gates[:, here] = pre
        extra_waits[block].wait()
        extras[:, here] = dot_nt(select, extra_in[block])
    width = gates.shape[1]

    def gate(kind):
        return gates[pl.ds(kind * MEMORY_HEADS + head, 1), :] + gate_bias[kind * MEMORY_HEADS + head]

    sub = lax.broadcasted_iota(jnp.int32, (8, width), 0)
    forget_f = log_sigmoid(gate(1)) + extras[pl.ds(head, 1), :]
    forget_b = log_sigmoid(gate(3)) + extras[pl.ds(MEMORY_HEADS + head, 1), :]
    decay_f = scan_lanes(jnp.broadcast_to(forget_f, (8, width)), jnp.add, 0.0, False)[0:1]
    decay_b = scan_lanes(jnp.broadcast_to(forget_b, (8, width)), jnp.add, 0.0, True)[0:1]
    level_f, level_b = gate(0) - decay_f, gate(2) - decay_b
    peak_f = scan_lanes(jnp.broadcast_to(level_f, (8, width)), jnp.maximum, LOW_START, False)[0:1]
    peak_b = scan_lanes(jnp.broadcast_to(level_b, (8, width)), jnp.maximum, LOW_START, True)[0:1]
    most_f = jnp.max(level_f, axis=1, keepdims=True)
    most_b = jnp.max(level_b, axis=1, keepdims=True)
    end_f, end_b = jnp.exp(level_f - most_f) * key_scale, jnp.exp(level_b - most_b) * key_scale
    vectors = [level_f, level_b, decay_f, decay_b, peak_f, peak_b, end_f, end_b]
    table = jnp.zeros((8, width), F32)
    for place, vector in enumerate(vectors):
        table = jnp.where(sub == place, vector, table)
    rows_out[...] = table


def front_kernel(dims, tab, *refs):
    group, blocks, rows, n_parts, n_pieces = dims
    parts, pieces = refs[:n_parts], refs[n_parts : n_parts + n_pieces]
    glu_out, head_out, tail_out, held, value_w, gate_w, part_sems, sems = refs[n_parts + n_pieces :]
    weight_waits = fetch_weights(tab, group, blocks, rows, pieces, (value_w, gate_w), sems)
    waits = fetch_parts(tab, group, parts, held, part_sems)
    arrived(weight_waits)
    count = held.shape[2]
    for block in range(group):
        arrived(waits[block])
        have = [held[place, block] for place in range(n_parts)]
        glu = (project(have, value_w) * jax.nn.sigmoid(project(have, gate_w))).astype(BF16)
        glu_out[block * count : (block + 1) * count, :] = glu
        if block == 0:
            head_out[...] = glu[0:HALO, :]
        if block == group - 1:
            tail_out[...] = glu[count - HALO :, :]


def states_kernel(dims, tab, *refs):
    group, blocks, rows, n_parts, n_pieces, quarters, n_sends = dims
    refs = list(refs)
    parts = [refs.pop(0) for _ in range(n_parts)]
    key_pieces = [refs.pop(0) for _ in range(n_pieces)]
    value_pieces = [refs.pop(0) for _ in range(n_pieces)]
    table_in, key_out, value_out = [refs.pop(0) for _ in range(3)]
    sends = [refs.pop(0) for _ in range(n_sends)]
    held, key_w, value_w, table, part_sems, sems = refs
    key_wait = fetch_weights(tab, group, blocks, rows, key_pieces, (key_w,), sems.at[pl.ds(0, 1)])
    value_wait = fetch_weights(tab, group, blocks, rows, value_pieces, (value_w,), sems.at[pl.ds(1, 1)])
    table_wait = fetch([(table_in, table, sems.at[2])])
    waits = fetch_parts(tab, group, parts, held, part_sems)
    arrived(key_wait)
    arrived(value_wait)
    arrived(table_wait)
    count = held.shape[2]
    columns = jnp.transpose(table[...])
    mats, sums = [None, None], [None, None]
    for block in range(group):
        here = slice(block * count, (block + 1) * count)
        arrived(waits[block])
        have = [held[place, block] for place in range(n_parts)]
        keys = project(have, key_w).astype(BF16)
        key_out[here, :] = keys
        values = project(have, value_w).astype(BF16)
        value_out[here, :] = values
        keys = keys.astype(F32)
        for place in range(2):
            weighted = keys * columns[here, 6 + place : 7 + place]
            line = jnp.sum(weighted, axis=0, keepdims=True)
            mat = dot_tn(weighted.astype(BF16), values)
            sums[place] = line if block == 0 else sums[place] + line
            mats[place] = mat if block == 0 else mats[place] + mat
    width = table.shape[1]
    at = lax.broadcasted_iota(jnp.int32, (TAIL, HEAD), 0)
    made = []
    for place, lane in ((0, width - 1), (1, 0)):
        total = table[2 + place : 3 + place, lane : lane + 1]
        most = table[4 + place : 5 + place, lane : lane + 1]
        lines = (*split3(sums[place]), *split3(total), *split3(total + most))
        tail = jnp.zeros((TAIL, HEAD), F32)
        for line, value in enumerate(lines):
            tail = jnp.where(at == line, value, tail)
        made.append((mats[place].astype(BF16), tail.astype(BF16)))
    for slot, send in enumerate(sends):
        if n_sends == quarters - 1 and quarters > 1:
            ahead = tab[3 * group] + slot + 1 < quarters
            for chosen, (mat, tail) in ((ahead, made[0]), (jnp.logical_not(ahead), made[1])):

                @pl.when(chosen)
                def _(mat=mat, tail=tail, send=send):
                    send[0:HEAD, :] = mat
                    send[HEAD:, :] = tail
        else:
            send[0:HEAD, :] = made[slot][0]
            send[HEAD:, :] = made[slot][1]


def local_kernel(dims, tab, *refs):
    group, blocks, rows, n_parts, n_pieces, key_scale = dims
    parts, pieces = refs[:n_parts], refs[n_parts : n_parts + n_pieces]
    keys_in, values_in, table_in = refs[n_parts + n_pieces : n_parts + n_pieces + 3]
    query_out, numer_f, numer_b, denom_out = refs[n_parts + n_pieces + 3 : n_parts + n_pieces + 7]
    held, query_w, keys, values, table, part_sems, sems = refs[n_parts + n_pieces + 7 :]
    weight_wait = fetch_weights(tab, group, blocks, rows, pieces, (query_w,), sems.at[pl.ds(3, 1)])
    waits = fetch_parts(tab, group, parts, held, part_sems)
    others_wait = fetch(
        [(keys_in, keys, sems.at[0]), (values_in, values, sems.at[1]), (table_in, table, sems.at[2])]
    )
    arrived(weight_wait)
    length = keys.shape[0]
    count = length // group
    spot_t = lax.broadcasted_iota(jnp.int32, (count, count), 0)
    spot_s = lax.broadcasted_iota(jnp.int32, (count, count), 1)
    masks = (spot_s <= spot_t, spot_s >= spot_t)
    lane = lax.broadcasted_iota(jnp.int32, (count, 128), 1)
    for block in range(group):
        here = slice(block * count, (block + 1) * count)
        arrived(waits[block])
        queries = project([held[place, block] for place in range(n_parts)], query_w).astype(BF16)
        query_out[here, :] = queries
        if block == 0:
            arrived(others_wait)
        raw = dot_nt(queries, keys[...]) * key_scale
        columns = jnp.transpose(table[:, here])
        denoms = []
        for way, out in enumerate((numer_f, numer_b)):
            top = columns[:, 4 + way : 5 + way]
            power = jnp.where(masks[way], table[way : way + 1, here] - top, LOW_START)
            scores = raw[:, here] * jnp.exp(power)
            denom = jnp.sum(scores, axis=1, keepdims=True)
            numer = dot(scores.astype(BF16), values[here, :])
            others = slice(0, block * count) if way == 0 else slice((block + 1) * count, length)
            if others.stop > others.start:
                scores = raw[:, others] * jnp.exp(table[way : way + 1, others] - top)
                denom = denom + jnp.sum(scores, axis=1, keepdims=True)
                numer = numer + dot(scores.astype(BF16), values[others, :])
            out[here, :] = numer.astype(BF16)
            denoms.append(denom)
        denom_out[here, :] = jnp.where(lane == 0, denoms[0], denoms[1])


def conv_kernel(tab, glu, before, after, taps, conv_out, stats_out, padded, sums):
    length, width = glu.shape
    padded[0:HALO, :] = before[...].astype(F32)
    padded[HALO : HALO + length, :] = glu[...].astype(F32)
    padded[HALO + length :, :] = after[...].astype(F32)
    chunk = 64
    lead = HALO - REACH
    lane = lax.broadcasted_iota(jnp.int32, (chunk, 128), 1)

    def one(step, carry):
        base = pl.multiple_of(step * chunk, chunk)
        line = jnp.zeros((chunk, 128), F32)
        square = jnp.zeros((chunk, 128), F32)
        for left in range(0, width, 128):
            lanes = slice(left, left + 128)
            total = jnp.zeros((chunk, 128), F32)
            window_all = padded[pl.ds(base, chunk + 32), lanes]
            for shift in range(8):
                window = pltpu.roll(window_all, chunk + 32 - shift, 0) if shift else window_all
                for high in range(4):
                    tap = 8 * high + shift - lead
                    if 0 <= tap < KW:
                        total = total + taps[tap : tap + 1, lanes] * window[8 * high : 8 * high + chunk, :]
            conv_out[pl.ds(base, chunk), lanes] = total
            line = line + total
            square = square + total * total
        line = jnp.sum(line, axis=1, keepdims=True)
        square = jnp.sum(square, axis=1, keepdims=True)
        sums[pl.ds(base, chunk), :] = jnp.where(lane == 0, line, square)
        return carry

    lax.fori_loop(0, length // chunk, one, 0)
    stats_out[...] = jnp.transpose(sums[...])[0:8, :]


def act_kernel(dims, tab, conv, *refs):
    group, channels, halves = dims
    stats, (gain, bias), outs = refs[:group], refs[group : group + 2], refs[group + 2 :]
    total = stats[0][...]
    for more in stats[1:]:
        total = total + more[...]
    mean = total[0:1, :] / channels
    var = total[1:2, :] / channels - mean * mean
    scale = lax.rsqrt(var + EPS)
    sub = lax.broadcasted_iota(jnp.int32, total.shape, 0)
    columns = jnp.transpose(jnp.where(sub == 0, mean, scale))
    count = outs[0].shape[0]
    for slot, out in enumerate(outs):
        which = tab[group + slot]
        start = pl.multiple_of(which * count, count)
        picked = columns[0:count, :]
        for block in range(1, group):
            picked = jnp.where(which == block, columns[block * count : (block + 1) * count, :], picked)
        normal = (conv[pl.ds(start, count), :] - picked[:, 0:1]) * picked[:, 1:2]
        normal = normal * gain[...] + bias[...]
        place_rows(tab, group, halves, out, (normal * jax.nn.sigmoid(normal)).astype(BF16))


def place_rows(tab, group, halves, out, value):
    if halves == 1:
        out[...] = value
        return
    half = value.shape[0] // 2
    own = tab[3 * group + 2]
    out[pl.ds(pl.multiple_of((1 - own) * half, half), half), :] = value[:half, :]
    out[pl.ds(pl.multiple_of(own * half, half), half), :] = value[half:, :]


def incoming(pieces):
    levels, best, passed = [], jnp.full((1, HEAD), LOW_START, F32), jnp.zeros((1, HEAD), F32)
    for piece, there in pieces:
        lines = piece[HEAD:, :].astype(F32)
        level = lines[6:7] + lines[7:8] + lines[8:9] + passed
        if there is not None:
            level = jnp.where(there, level, LOW_START)
        levels.append(level)
        best = jnp.maximum(best, level)
        passed = passed + lines[3:4] + lines[4:5] + lines[5:6]
    mat, vec = jnp.zeros((HEAD, HEAD), F32), jnp.zeros((1, HEAD), F32)
    for (piece, there), level in zip(pieces, levels):
        weight = jnp.exp(level - best)
        if there is not None:
            weight = jnp.where(there, weight, 0.0)
        lines = piece[HEAD:, :].astype(F32)
        mat = mat + weight * piece[0:HEAD, :].astype(F32)
        vec = vec + weight * (lines[0:1] + lines[1:2] + lines[2:3])
    return mat, vec, best


def finish_kernel(dims, tab, *refs):
    group, n_states, ringed, halves = dims
    queries_in, numer_f, numer_b, denoms_in, table_in = refs[:5]
    states_in, gain = refs[5 : 5 + n_states], refs[5 + n_states]
    outs = refs[6 + n_states : 6 + n_states + group]
    states, table, queries_all, numers, denoms_all, result, sems, block_sems = refs[6 + n_states + group :]
    length = queries_in.shape[0]
    count = length // group
    first = fetch(
        [(state, states.at[slot], sems.at[slot]) for slot, state in enumerate(states_in)]
        + [(table_in, table, sems.at[n_states])]
    )
    waits = []
    for block in range(group):
        here = pl.ds(block * count, count)
        waits.append(
            fetch(
                [
                    (queries_in.at[here, :], queries_all.at[here, :], block_sems.at[block, 0]),
                    (numer_f.at[here, :], numers.at[0, here, :], block_sems.at[block, 1]),
                    (numer_b.at[here, :], numers.at[1, here, :], block_sems.at[block, 2]),
                    (denoms_in.at[here, :], denoms_all.at[here, :], block_sems.at[block, 3]),
                ]
            )
        )
    arrived(first)
    pieces = [states.at[slot] for slot in range(n_states)]
    if ringed:
        at = tab[3 * group]
        ahead = [(state, slot + 1 <= at) for slot, state in enumerate(pieces)]
        back = [(state, slot + 1 > at) for slot, state in enumerate(pieces)][::-1]
    else:
        ahead, back = [(pieces[0], None)], [(pieces[1], None)]
    mats, vecs, bests = [], [], []
    for these in (ahead, back):
        mat, vec, best = incoming(these)
        high = mat.astype(BF16)
        mats.append((high, (mat - high.astype(F32)).astype(BF16)))
        vecs.append(vec)
        bests.append(best[:, 0:1])
    line = lax.broadcasted_iota(jnp.int32, (128, HEAD), 0)
    vec = jnp.where(line == 0, vecs[0], vecs[1])
    vec_high = vec.astype(BF16)
    vec_low = (vec - vec_high.astype(F32)).astype(BF16)
    sub = lax.broadcasted_iota(jnp.int32, (8, length), 0)
    peak = jnp.where(sub == 0, table[4:5, :], table[5:6, :])
    decay = jnp.where(sub == 0, table[2:3, :], table[3:4, :])
    best = jnp.where(sub == 0, bests[0], bests[1])
    top = jnp.maximum(peak, best)
    carry = jnp.transpose(jnp.exp(best - top))
    stay = jnp.transpose(jnp.exp(peak - top))
    floor = jnp.transpose(jnp.exp(-(decay + top)))
    for block in range(group):
        here = slice(block * count, (block + 1) * count)
        arrived(waits[block])
        queries = queries_all[here, :]
        along = (dot_nt(queries, vec_high) + dot_nt(queries, vec_low))[:, 0:8]
        denom = stay[here, :] * denoms_all[here, 0:8] + carry[here, :] * along
        inverse = 1.0 / jnp.maximum(jnp.abs(denom), floor[here, :])
        left, right = stay[here, :] * inverse, carry[here, :] * inverse
        summed = None
        for way, (high, low) in enumerate(mats):
            term = left[:, way : way + 1] * numers[way, here, :].astype(F32)
            term = term + right[:, way : way + 1] * (dot(queries, high) + dot(queries, low))
            summed = term if summed is None else summed + term
        scale = lax.rsqrt(jnp.mean(summed * summed, axis=1, keepdims=True) + EPS)
        result[here, :] = (summed * scale * gain[...]).astype(BF16)
    for slot, out in enumerate(outs):
        start = pl.multiple_of(tab[group + slot] * count, count)
        place_rows(tab, group, halves, out, result[pl.ds(start, count), :])


def compose_line(total, level, mat, vec):
    tail = jnp.concatenate([jnp.broadcast_to(x[None, :], (1, HEAD)) for x in (*split3(vec), *split3(total + jnp.zeros((HEAD,), F32)), *split3(level + jnp.zeros((HEAD,), F32)))])
    tail = jnp.concatenate([tail, jnp.zeros((TAIL - tail.shape[0], HEAD), F32)])
    return jnp.concatenate([mat, tail]).astype(BF16)


def shards(
    tokens,
    norm_gain,
    glu_value,
    glu_gate,
    conv_taps,
    ln_gain,
    ln_bias,
    query_weight,
    key_weight,
    value_weight,
    gate_weight,
    gate_bias,
    log_decay_extra,
    mem_gain,
    out_conv,
    out_mem,
):
    sp, tp = lax.axis_size("sp"), lax.axis_size("tp")
    group = mem_gain.shape[0] // HEAD
    quarters = sp // group
    count = tokens.shape[0]
    length = group * count
    rows = key_weight.shape[0]
    features = norm_gain.shape[0]
    channels = conv_taps.shape[1] // group
    conv_all = channels * group * tp
    blocks = sp
    key_scale = HEAD ** (-0.5)
    me, core = lax.axis_index("sp"), lax.axis_index("tp")
    place, quarter = me % group, me // group
    paired = tp == 2
    even = group & (group - 1) == 0
    ringed = quarters <= RING_MOST

    def source(p, slot):
        return p ^ slot if even else (p - slot) % group

    def target(p, slot):
        return p ^ slot if even else (p + slot) % group

    def in_plane(x, slot):
        if slot == 0:
            return x
        pairs = [(i, i - i % group + target(i % group, slot)) for i in range(sp)]
        return lax.ppermute(x, "sp", pairs)

    def along(x, hops, ring=False):
        pairs = [(i, i + hops * group) for i in range(sp)]
        pairs = [(i, j % sp) for i, j in pairs] if ring else [(i, j) for i, j in pairs if 0 <= j < sp]
        return lax.ppermute(x, "sp", pairs)

    def swap(x):
        return lax.ppermute(x, "tp", [(0, 1), (1, 0)])

    lines = [[k * group + j for k in range(quarters)] for j in range(group)]

    def tall(x):
        return jnp.concatenate(x, axis=0) if len(x) > 1 else x[0]

    def split_weights(weights, width):
        got = []
        for slot in range(group):
            to = target(place, slot) * width
            sent = tall([lax.dynamic_slice_in_dim(weight, to, width, 1) for weight in weights])
            got.append(in_plane(sent, slot))
        return got

    def ring(piece):
        if not ringed:
            return [lax.all_gather(piece, "sp", axis=0, tiled=True, axis_index_groups=lines)]
        pieces = [piece]
        for _ in range(1, quarters):
            pieces.append(along(pieces[-1], 1, True))
        return pieces

    slots = list(range(group))
    sources = [source(place, slot) for slot in slots]
    targets = [target(place, slot) for slot in slots]
    inverse = [p ^ place if even else (place - p) % group for p in slots]
    shift = core * tokens.shape[1] if paired else 0
    offsets = []
    for hop in range(quarters):
        block_quarter = (quarter - hop) % quarters if ringed else hop
        for slot in slots:
            offsets.append(((block_quarter * group + sources[slot]) * rows - shift) % features)
    head = core * group + place
    entries = (*sources, *targets, *inverse, quarter, 0, core, place, head, *offsets)
    tab = jnp.stack([jnp.asarray(x, jnp.int32) for x in entries])

    got = split_weights([glu_value, glu_gate, key_weight], channels)
    glu_piece = tall([x[: 2 * rows] for x in got])
    key_piece = tall([x[2 * rows :] for x in got])
    wide = tokens.astype(F32)
    squares = jnp.sum(wide * wide, axis=-1, keepdims=True)
    squares = squares + swap(squares) if paired else lax.psum(squares, "tp")
    own_gain = lax.dynamic_slice_in_dim(norm_gain, core * tokens.shape[1], tokens.shape[1], 0)
    normed = (wide * lax.rsqrt(squares / features + EPS) * own_gain).astype(BF16)
    extras = [part.astype(BF16) for part in split3(log_decay_extra)]
    extras = jnp.pad(jnp.concatenate(extras, 1), ((0, 0), (0, 128 - 3 * 2 * MEMORY_HEADS)))
    own_width = tokens.shape[1]
    payload = jnp.concatenate([normed, extras], 1)
    payload = tall([in_plane(payload, slot) for slot in slots])
    if paired:
        parts, extra_at = [payload, swap(payload)], own_width // 128
        extra = payload
        part_width = own_width
    else:
        parts, extra_at = [lax.all_gather(payload[:, :own_width], "tp", axis=1, tiled=True)], 0
        extra = payload[:, own_width:]
        part_width = features
    glu_pieces = ring(glu_piece)
    got = split_weights([value_weight, query_weight], HEAD)
    value_piece, query_piece = [tall([x[m * rows : (m + 1) * rows] for x in got]) for m in range(2)]
    conv_rows = tall([lax.dynamic_slice_in_dim(out_conv, at * channels, channels, 0) for at in sources])
    mem_rows = tall([lax.dynamic_slice_in_dim(out_mem, at * HEAD, HEAD, 0) for at in sources])
    key_pieces = ring(key_piece)
    value_pieces = ring(value_piece)
    query_pieces = ring(query_piece)

    def far(arrays):
        return [pl.BlockSpec(memory_space=pl.ANY) for _ in arrays]

    def wholes(shapes):
        return [whole(x.shape) for x in shapes]

    def dma(*dims):
        return pltpu.SemaphoreType.DMA(dims)

    def call(kernel, in_specs, out_specs, out_shape, scratch, flops, steps=1):
        return pl.pallas_call(
            kernel,
            grid_spec=pltpu.PrefetchScalarGridSpec(
                num_scalar_prefetch=1,
                grid=(steps,),
                in_specs=in_specs,
                out_specs=out_specs,
                scratch_shapes=scratch,
            ),
            out_shape=out_shape,
            compiler_params=params(),
            cost_estimate=pl.CostEstimate(flops=flops, transcendentals=0, bytes_accessed=4 << 20),
        )

    def shape(dims, kind=BF16):
        return jax.ShapeDtypeStruct(dims, kind)

    n_parts, n_pieces = len(parts), len(key_pieces)
    halves = 2 if paired else 1
    work = 2 * length * features * HEAD
    held = [pltpu.VMEM((n_parts, group, count, part_width), BF16)]
    part_sems = [dma(group * n_parts)]
    square = [pltpu.VMEM((features, HEAD), BF16)]
    table = call(
        functools.partial(gates_kernel, (group, n_parts, extra_at, key_scale)),
        far(parts) + far([extra, gate_weight]) + [pl.BlockSpec(memory_space=pltpu.SMEM)],
        whole((8, length)),
        shape((8, length), F32),
        held
        + [pltpu.VMEM((group, count, 128), BF16), pltpu.VMEM((4 * MEMORY_HEADS, features), BF16)]
        + [pltpu.VMEM((4 * MEMORY_HEADS, length), F32), pltpu.VMEM((2 * MEMORY_HEADS, length), F32)]
        + part_sems
        + [dma(group + 1)],
        work,
    )(tab, *parts, extra, gate_weight.T, gate_bias)

    made = [shape((length, channels)), shape((HALO, channels)), shape((HALO, channels))]
    glu, glu_head, glu_tail = call(
        functools.partial(front_kernel, (group, blocks, rows, n_parts, n_pieces)),
        far(parts) + far(glu_pieces),
        wholes(made),
        made,
        held + [pltpu.VMEM((features, channels), BF16)] * 2 + part_sems + [dma(2)],
        2 * work,
    )(tab, *parts, *glu_pieces)

    glu_before = along(glu_tail, 1)
    glu_after = along(glu_head, -1)

    def own_lanes(lines, width):
        return pl.BlockSpec((lines, width), lambda i, tab: (0, tab[3 * group + 3]))

    conv, stats = call(
        conv_kernel,
        [whole((length, channels)), whole((HALO, channels)), whole((HALO, channels)), own_lanes(KW, channels)],
        [whole((length, channels)), whole((8, length))],
        [shape((length, channels), F32), shape((8, length), F32)],
        [pltpu.VMEM((length + 2 * HALO, channels), F32), pltpu.VMEM((length, 128), F32)],
        2 * work,
        1,
    )(tab, glu, glu_before, glu_after, conv_taps)
    stats = stats + swap(stats) if paired else lax.psum(stats, "tp")
    all_stats = [in_plane(stats, slot) for slot in slots]
    acts = call(
        functools.partial(act_kernel, (group, conv_all, halves)),
        [whole((length, channels))] + [whole((8, length))] * group + [own_lanes(1, channels)] * 2,
        [whole((count, channels))] * group,
        [shape((count, channels))] * group,
        [],
        work,
        1,
    )(tab, conv, *all_stats, ln_gain[None, :], ln_bias[None, :])
    acts = [in_plane(act, slot) for slot, act in enumerate(acts)]

    n_sends = quarters - 1 if ringed else 2
    made = [shape((length, HEAD))] * 2 + [shape((HEAD + TAIL, HEAD))] * n_sends
    keys, values, *sends = call(
        functools.partial(states_kernel, (group, blocks, rows, n_parts, n_pieces, quarters, n_sends)),
        far(parts) + far(key_pieces) + far(value_pieces) + far([table]),
        wholes(made),
        made,
        held + square * 2 + [pltpu.VMEM((8, length), F32)] + part_sems + [dma(3)],
        2 * work,
    )(tab, *parts, *key_pieces, *value_pieces, table)
    if ringed:
        states = [along(send, hop + 1, True) for hop, send in enumerate(sends)]
    else:
        states = far_states(sends[0], sends[1], quarter, quarters, lines)

    tall_head = [pltpu.VMEM((length, HEAD), BF16)]
    made = [shape((length, HEAD))] * 3 + [shape((length, 128), F32)]
    locals_made = call(
        functools.partial(local_kernel, (group, blocks, rows, n_parts, n_pieces, key_scale)),
        far(parts) + far(query_pieces) + far([keys, values, table]),
        wholes(made),
        made,
        held + square + tall_head * 2 + [pltpu.VMEM((8, length), F32)] + part_sems + [dma(4)],
        work,
    )(tab, *parts, *query_pieces, keys, values, table)

    made = [shape((count, HEAD))] * group
    memories = call(
        functools.partial(finish_kernel, (group, len(states), ringed, halves)),
        far(locals_made) + far([table]) + far(states) + [own_lanes(1, HEAD)],
        wholes(made),
        made,
        [pltpu.VMEM((len(states), HEAD + TAIL, HEAD), BF16), pltpu.VMEM((8, length), F32)]
        + tall_head
        + [pltpu.VMEM((2, length, HEAD), BF16), pltpu.VMEM((length, 128), F32)]
        + tall_head
        + [dma(len(states) + 1), dma(group, 4)],
        work,
    )(tab, *locals_made, table, *states, mem_gain[None, :])
    memories = [in_plane(memory, slot) for slot, memory in enumerate(memories)]

    partial = dot(jnp.concatenate(acts, 1), conv_rows)
    result = (partial + dot(jnp.concatenate(memories, 1), mem_rows)).astype(BF16)
    if paired:
        half = count // 2
        return (result[half:].astype(F32) + swap(result[:half]).astype(F32)).astype(BF16)
    return lax.psum_scatter(result, "tp", scatter_dimension=0, tiled=True)


def far_states(state_f, state_b, quarter, quarters, lines):
    found = []
    for state, reverse in ((state_f, False), (state_b, True)):
        pieces = lax.all_gather(state, "sp", axis_index_groups=lines).astype(F32)
        if reverse:
            pieces = jnp.flip(pieces, 0)
        at = quarters - 1 - quarter if reverse else quarter
        totals = pieces[:, HEAD + 3, 0] + pieces[:, HEAD + 4, 0] + pieces[:, HEAD + 5, 0]
        levels = pieces[:, HEAD + 6, 0] + pieces[:, HEAD + 7, 0] + pieces[:, HEAD + 8, 0]
        order = jnp.arange(quarters)
        between = (order[None, :] > order[:, None]) & (order[None, :] < at)
        levels = levels + jnp.sum(jnp.where(between, totals[None, :], 0.0), axis=1)
        levels = jnp.where(order < at, levels, LOW_START)
        best = jnp.max(levels)
        weights = jnp.exp(levels - best)
        mat = jnp.sum(weights[:, None, None] * pieces[:, :HEAD], axis=0)
        vec = jnp.sum(weights[:, None] * (pieces[:, HEAD] + pieces[:, HEAD + 1] + pieces[:, HEAD + 2]), axis=0)
        found.append(compose_line(jnp.zeros((), F32), best, mat, vec))
    return found


def solution(mesh):
    in_specs = (
        P("sp", "tp"),
        P(),
        P("sp", "tp"),
        P("sp", "tp"),
        P(None, "tp"),
        P("tp"),
        P("tp"),
        P("sp", "tp"),
        P("sp", "tp"),
        P("sp", "tp"),
        P(),
        P(),
        P("sp", None),
        P("tp"),
        P("tp", None),
        P("tp", None),
    )
    out_specs = P(("sp", "tp"), None)

    return jax.shard_map(shards, mesh=mesh, in_specs=in_specs, out_specs=out_specs, check_vma=False)
```

profile of v0, /device:TPU:0, one launch (start us, length us, event | category | flops | bytes accessed | tf_op | source)
XLA Modules:
  0.0 199.4 jit_solution(7642410620452838970)
XLA Ops:
  3.6 1.7 constant_dynamic-slice_fusion.5
  7.5 2.6 %collective-permute-start.1 = (bf16[256,1152]{1,0:T(8,128)(2,1)S(1)}, bf16[256,1152]{1,0:T(8,128)(2,1)S(1)}, u32[]{:S(2)}, u32[]{:S(2)}) collective-permute-start(bf16[256,1152]{1,0:T(8,128)(2,1)S(1)} %pad_maximum_fusion.1), channel_id=1, source_target_pairs={{0,2},{2,0},{4,6},{6,4},{8,10},{10,8},{12,14},{14,12},{16,18},{18,... | collective-permute-start | bytes 1769480 | tf_op jit(solution)/shard_map/ppermute | solution.py:508
  11.7 2.0 %collective-permute-start.5 = (bf16[384,256]{1,0:T(8,128)(2,1)S(1)}, bf16[384,256]{1,0:T(8,128)(2,1)S(1)}, u32[]{:S(2)}, u32[]{:S(2)}) collective-permute-start(bf16[384,256]{1,0:T(8,128)(2,1)S(1)} %pad_maximum_fusion.5), channel_id=1, source_target_pairs={{0,2},{2,0},{4,6},{6,4},{8,10},{10,8},{12,14},{14,12},{16,18},{18,... | collective-permute-start | bytes 589832 | tf_op jit(solution)/shard_map/ppermute | solution.py:508
  13.8 1.6 collective-permute-start.6
  15.4 8.9 %collective-permute-done.1 = bf16[256,1152]{1,0:T(8,128)(2,1)S(1)} collective-permute-done((bf16[256,1152]{1,0:T(8,128)(2,1)S(1)}, bf16[256,1152]{1,0:T(8,128)(2,1)S(1)}, u32[]{:S(2)}, u32[]{:S(2)}) %collective-permute-start.1) | collective-permute-done | bytes 589856 | tf_op jit(solution)/shard_map/ppermute | solution.py:508
  24.3 3.0 %collective-permute-start.7 = (bf16[384,256]{1,0:T(8,128)(2,1)S(1)}, bf16[384,256]{1,0:T(8,128)(2,1)S(1)}, u32[]{:S(2)}, u32[]{:S(2)}) collective-permute-start(bf16[384,256]{1,0:T(8,128)(2,1)S(1)} %pad_maximum_fusion.7), channel_id=1, source_target_pairs={{0,6},{2,4},{4,2},{6,0},{8,14},{10,12},{12,10},{14,8},{16,22},{18,... | collective-permute-start | bytes 589832 | tf_op jit(solution)/shard_map/ppermute | solution.py:508
  27.2 11.7 %collective-permute-done.2 = bf16[256,1152]{1,0:T(8,128)(2,1)S(1)} collective-permute-done((bf16[256,1152]{1,0:T(8,128)(2,1)S(1)}, bf16[256,1152]{1,0:T(8,128)(2,1)S(1)}, u32[]{:S(2)}, u32[]{:S(2)}) %collective-permute-start.2) | collective-permute-done | bytes 589856 | tf_op jit(solution)/shard_map/ppermute | solution.py:508
  38.9 2.1 %collective-permute-start.21 = (bf16[256,256]{1,0:T(8,128)(2,1)S(1)}, bf16[256,256]{1,0:T(8,128)(2,1)S(1)}, u32[]{:S(2)}, u32[]{:S(2)}) collective-permute-start(bf16[256,256]{1,0:T(8,128)(2,1)S(1)} %pad_maximum_fusion.9), channel_id=1, source_target_pairs={{0,4},{2,6},{4,0},{6,2},{8,12},{10,14},{12,8},{14,10},{16,20},{18,... | collective-permute-start | bytes 393224 | tf_op jit(solution)/shard_map/ppermute | solution.py:508
  41.0 4.5 %pad_maximum_fusion.refs_0_.refs_2_ = bf16[1024,1152]{1,0:T(8,128)(2,1)S(1)} fusion(bf16[256,1152]{1,0:T(8,128)(2,1)S(1)} %collective-permute-done.3, bf16[256,1152]{1,0:T(8,128)(2,1)S(1)} %collective-permute-done.2, bf16[256,1152]{1,0:T(8,128)(2,1)S(1)} %collective-permute-done.1, bf16[256,128]{1,0:T(8,128)(2,1)S(1)} %pad.4, bf16[256,1024]{1,0:T(8,128)(2,1)S(1)} %fusion.24), kind=kLoop, calls=%fused_computation.18 | loop fusion | flops 11796480 | bytes 4718592 | tf_op jit(solution)/shard_map/concatenate | solution.py:521
  45.6 1.8 collective-permute-done.6
  47.4 1.6 collective-permute-start.8
  50.6 11.2 %collective-permute-done.8.refs_3_ = bf16[1024,256]{1,0:T(8,128)(2,1)S(1)} collective-permute-done((bf16[1024,256]{1,0:T(8,128)(2,1)S(1)}, bf16[1024,256]{1,0:T(8,128)(2,1)S(1)}, u32[]{:S(2)}, u32[]{:S(2)}) %collective-permute-start.8) | collective-permute-done | bytes 524320 | tf_op jit(solution)/shard_map/ppermute | solution.py:513
  63.3 1.6 collective-permute-start.23
  65.0 2.1 %collective-permute-start.26 = (bf16[512,256]{1,0:T(8,128)(2,1)S(1)}, bf16[512,256]{1,0:T(8,128)(2,1)}, u32[]{:S(2)}, u32[]{:S(2)}) collective-permute-start(bf16[512,256]{1,0:T(8,128)(2,1)S(1)} %pad_maximum_fusion.3.refs_2_), channel_id=1, source_target_pairs={{0,8},{2,10},{4,12},{6,14},{8,16},{10,18},{12,20},{14,22},{16,24},... | collective-permute-start | bytes 786440 | tf_op jit(solution)/shard_map/ppermute | solution.py:513
  67.1 11.4 %collective-permute-done.9.refs_4_ = bf16[1024,256]{1,0:T(8,128)(2,1)} collective-permute-done((bf16[1024,256]{1,0:T(8,128)(2,1)S(1)}, bf16[1024,256]{1,0:T(8,128)(2,1)}, u32[]{:S(2)}, u32[]{:S(2)}) %collective-permute-start.9) | collective-permute-done | bytes 524320 | tf_op jit(solution)/shard_map/ppermute | solution.py:513
  78.7 5.5 %collective-permute-done.29.refs_7_ = bf16[512,256]{1,0:T(8,128)(2,1)} collective-permute-done((bf16[512,256]{1,0:T(8,128)(2,1)S(1)}, bf16[512,256]{1,0:T(8,128)(2,1)}, u32[]{:S(2)}, u32[]{:S(2)}) %collective-permute-start.29) | collective-permute-done | bytes 262176 | tf_op jit(solution)/shard_map/ppermute | solution.py:513
  84.2 5.5 %collective-permute-done.23.refs_3_ = bf16[512,256]{1,0:T(8,128)(2,1)S(1)} collective-permute-done((bf16[512,256]{1,0:T(8,128)(2,1)S(1)}, bf16[512,256]{1,0:T(8,128)(2,1)S(1)}, u32[]{:S(2)}, u32[]{:S(2)}) %collective-permute-start.23) | collective-permute-done | bytes 262176 | tf_op jit(solution)/shard_map/ppermute | solution.py:513
  89.7 5.7 %collective-permute-done.26.refs_3_ = bf16[512,256]{1,0:T(8,128)(2,1)} collective-permute-done((bf16[512,256]{1,0:T(8,128)(2,1)S(1)}, bf16[512,256]{1,0:T(8,128)(2,1)}, u32[]{:S(2)}, u32[]{:S(2)}) %collective-permute-start.26) | collective-permute-done | bytes 262176 | tf_op jit(solution)/shard_map/ppermute | solution.py:513
  95.4 2.7 %constant_dynamic-slice_fusion.3 = (bf16[256,2048]{1,0:T(8,128)(2,1)S(1)}, bf16[256,2048]{1,0:T(8,128)(2,1)S(1)}, bf16[256,2048]{1,0:T(8,128)(2,1)S(1)}, bf16[256,2048]{1,0:T(8,128)(2,1)S(1)}) fusion(bf16[1024,2048]{1,0:T(8,128)(2,1)} %param.31, s32[]{:T(128)S(6)} %select_n.153, s32[]{:T(128)S(6)} %select_n.154, s32[]{:T(128)S(6)} %select_n.156, ...), kind=kLoop, calls=%fused_computation.61 | loop fusion | bytes 8388624 | tf_op jit(solution)/shard_map/dynamic_slice | solution.py:578
  98.2 14.0 %collective-permute-done.30.refs_8_ = bf16[512,256]{1,0:T(8,128)(2,1)S(1)} collective-permute-done((bf16[512,256]{1,0:T(8,128)(2,1)}, bf16[512,256]{1,0:T(8,128)(2,1)S(1)}, u32[]{:S(2)}, u32[]{:S(2)}) %collective-permute-start.30) | collective-permute-done | bytes 262176 | tf_op jit(solution)/shard_map/ppermute | solution.py:513
  112.2 5.6 %collective-permute-done.24.refs_4_ = bf16[512,256]{1,0:T(8,128)(2,1)S(1)} collective-permute-done((bf16[512,256]{1,0:T(8,128)(2,1)S(1)}, bf16[512,256]{1,0:T(8,128)(2,1)S(1)}, u32[]{:S(2)}, u32[]{:S(2)}) %collective-permute-start.24) | collective-permute-done | bytes 262176 | tf_op jit(solution)/shard_map/ppermute | solution.py:513
  117.8 5.6 %collective-permute-done.27.refs_4_ = bf16[512,256]{1,0:T(8,128)(2,1)S(1)} collective-permute-done((bf16[512,256]{1,0:T(8,128)(2,1)}, bf16[512,256]{1,0:T(8,128)(2,1)S(1)}, u32[]{:S(2)}, u32[]{:S(2)}) %collective-permute-start.27) | collective-permute-done | bytes 262176 | tf_op jit(solution)/shard_map/ppermute | solution.py:513
  123.5 6.4 %shard_map.154 = (bf16[1024,256]{1,0:T(8,128)(2,1)S(1)}, bf16[16,256]{1,0:T(8,128)(2,1)S(1)}, bf16[16,256]{1,0:T(8,128)(2,1)S(1)}) custom-call(s32[33]{0:T(128)S(1)} %stack.104.tab, bf16[1024,1152]{1,0:T(8,128)(2,1)S(1)} %pad_maximum_fusion.refs_0_.refs_2_, bf16[1024,1152]{1,0:T(8,128)(2,1)} %collective-permute-done.4.refs_1_, ...), custom_call_target="tpu_custom_call" | custom-call | flops 2147483648 | bytes 4194304 | tf_op jit(solution)/shard_map/pallas_call | solution.py:630
  132.7 6.6 %shard_map.157.refs_10_.refs_8_.refs_4_ = f32[8,1024]{1,0:T(8,128)S(1)} custom-call(s32[33]{0:T(128)S(1)} %stack.104.tab, bf16[1024,1152]{1,0:T(8,128)(2,1)S(1)} %pad_maximum_fusion.refs_0_.refs_2_, bf16[1024,1152]{1,0:T(8,128)(2,1)} %collective-permute-done.4.refs_1_, bf16[1024,1152]{1,0:T(8,128)(2,1)S(1)} %pad_maximum_fusion.refs_0_.refs_2_, ...), custom_call_target="tpu_custom_call" | custom-call | flops 1073741824 | bytes 4194304 | tf_op jit(solution)/shard_map/pallas_call | solution.py:616
  139.4 7.6 %shard_map.158 = (bf16[1024,256]{1,0:T(8,128)(2,1)S(1)}, bf16[1024,256]{1,0:T(8,128)(2,1)S(1)}, bf16[272,256]{1,0:T(8,128)(2,1)S(1)}, bf16[272,256]{1,0:T(8,128)(2,1)S(1)}, bf16[272,256]{1,0:T(8,128)(2,1)S(1)}) custom-call(s32[33]{0:T(128)S(1)} %stack.104.tab, bf16[1024,1152]{1,0:T(8,128)(2,1)S(1)} %pad_maximum_fusion.refs_0_.refs_2_, ...), custom_call_target="tpu_custom_call" | custom-call | flops 2147483648 | bytes 4194304 | tf_op jit(solution)/shard_map/pallas_call | solution.py:669
  147.0 2.7 %collective-permute-start.32 = (bf16[272,256]{1,0:T(8,128)(2,1)S(1)}, bf16[272,256]{1,0:T(8,128)(2,1)S(1)}, u32[]{:S(2)}, u32[]{:S(2)}) collective-permute-start(bf16[272,256]{1,0:T(8,128)(2,1)S(1)} %get-tuple-element.42), channel_id=1, source_target_pairs={{0,8},{2,10},{4,12},{6,14},{8,16},{10,18},{12,20},{14,22},{16,24},... | collective-permute-start | bytes 417800 | tf_op jit(solution)/shard_map/ppermute | solution.py:513
  149.7 4.9 %collective-permute-start.33 = (bf16[272,256]{1,0:T(8,128)(2,1)S(1)}, bf16[272,256]{1,0:T(8,128)(2,1)S(1)}, u32[]{:S(2)}, u32[]{:S(2)}) collective-permute-start(bf16[272,256]{1,0:T(8,128)(2,1)S(1)} %get-tuple-element.43), channel_id=1, source_target_pairs={{0,16},{2,18},{4,20},{6,22},{8,24},{10,26},{12,28},{14,30},{16,0},... | collective-permute-start | bytes 417800 | tf_op jit(solution)/shard_map/ppermute | solution.py:513
  155.5 5.3 %shard_map.155 = (f32[1024,256]{1,0:T(8,128)S(1)}, f32[8,1024]{1,0:T(8,128)S(1)}) custom-call(s32[33]{0:T(128)S(1)} %stack.104.tab, bf16[1024,256]{1,0:T(8,128)(2,1)S(1)} %get-tuple-element.27.glu, bf16[16,256]{1,0:T(8,128)(2,1)S(1)} %collective-permute-done.11.before, bf16[16,256]{1,0:T(8,128)(2,1)S(1)} %collective-permute-done.12.after, ...), custom_call_target="tpu_custom_call" | custom-call | flops 2147483648 | bytes 4194304 | tf_op jit(solution)/shard_map/pallas_call | solution.py:645
  160.9 8.7 %shard_map.159 = (bf16[1024,256]{1,0:T(8,128)(2,1)S(1)}, bf16[1024,256]{1,0:T(8,128)(2,1)S(1)}, bf16[1024,256]{1,0:T(8,128)(2,1)S(1)}, f32[1024,128]{1,0:T(8,128)S(1)}) custom-call(s32[33]{0:T(128)S(1)} %stack.104.tab, bf16[1024,1152]{1,0:T(8,128)(2,1)S(1)} %pad_maximum_fusion.refs_0_.refs_2_, bf16[1024,1152]{1,0:T(8,128)(2,1)} %collective-permute-done.4.refs_1_, ...), custom_call_target="tpu_custom_call" | custom-call | flops 1073741824 | bytes 4194304 | tf_op jit(solution)/shard_map/pallas_call | solution.py:684
  173.2 7.1 %shard_map.160 = (bf16[256,256]{1,0:T(8,128)(2,1)S(1)}, bf16[256,256]{1,0:T(8,128)(2,1)S(1)}, bf16[256,256]{1,0:T(8,128)(2,1)S(1)}, bf16[256,256]{1,0:T(8,128)(2,1)S(1)}) custom-call(s32[33]{0:T(128)S(1)} %stack.104.tab, bf16[1024,256]{1,0:T(8,128)(2,1)S(1)} %get-tuple-element.38.refs_0_, bf16[1024,256]{1,0:T(8,128)(2,1)S(1)} %get-tuple-element.39.refs_1_, ...), custom_call_target="tpu_custom_call" | custom-call | flops 1073741824 | bytes 4194304 | tf_op jit(solution)/shard_map/pallas_call | solution.py:694
  192.4 2.7 %collective-permute-done.18 = bf16[256,256]{1,0:T(8,128)(2,1)S(1)} collective-permute-done((bf16[256,256]{1,0:T(8,128)(2,1)S(1)}, bf16[256,256]{1,0:T(8,128)(2,1)S(1)}, u32[]{:S(2)}, u32[]{:S(2)}) %collective-permute-start.18) | collective-permute-done | bytes 131104 | tf_op jit(solution)/shard_map/ppermute | solution.py:508
  196.6 1.9 collective-permute-done.38
  (120 shorter events, 32.5 us)
Async XLA Ops:
  7.5 16.8 %collective-permute-start.1 = (bf16[256,1152]{1,0:T(8,128)(2,1)S(1)}, bf16[256,1152]{1,0:T(8,128)(2,1)S(1)}, u32[]{:S(2)}, u32[]{:S(2)}) collective-permute-start(bf16[256,1152]{1,0:T(8,128)(2,1)S(1)} %pad_maximum_fusion.1), channel_id=1, source_target_pairs={{0,2},{2,0},{4,6},{6,4},{8,10},{10,8},{12,14},{14,12},{16,18},{18,... | collective-permute-start | bytes 1769480 | tf_op jit(solution)/shard_map/ppermute | solution.py:508
  10.1 28.8 %collective-permute-start.2 = (bf16[256,1152]{1,0:T(8,128)(2,1)S(1)}, bf16[256,1152]{1,0:T(8,128)(2,1)S(1)}, u32[]{:S(2)}, u32[]{:S(2)}) collective-permute-start(bf16[256,1152]{1,0:T(8,128)(2,1)S(1)} %pad_maximum_fusion.1), channel_id=1, source_target_pairs={{0,4},{2,6},{4,0},{6,2},{8,12},{10,14},{12,8},{14,10},{16,20},{18,... | collective-permute-start | bytes 1769480 | tf_op jit(solution)/shard_map/ppermute | solution.py:508
  11.6 27.3 %collective-permute-start.3 = (bf16[256,1152]{1,0:T(8,128)(2,1)S(1)}, bf16[256,1152]{1,0:T(8,128)(2,1)S(1)}, u32[]{:S(2)}, u32[]{:S(2)}) collective-permute-start(bf16[256,1152]{1,0:T(8,128)(2,1)S(1)} %pad_maximum_fusion.1), channel_id=1, source_target_pairs={{0,6},{2,4},{4,2},{6,0},{8,14},{10,12},{12,10},{14,8},{16,22},{18,... | collective-permute-start | bytes 1769480 | tf_op jit(solution)/shard_map/ppermute | solution.py:508
  11.7 33.8 %collective-permute-start.5 = (bf16[384,256]{1,0:T(8,128)(2,1)S(1)}, bf16[384,256]{1,0:T(8,128)(2,1)S(1)}, u32[]{:S(2)}, u32[]{:S(2)}) collective-permute-start(bf16[384,256]{1,0:T(8,128)(2,1)S(1)} %pad_maximum_fusion.5), channel_id=1, source_target_pairs={{0,2},{2,0},{4,6},{6,4},{8,10},{10,8},{12,14},{14,12},{16,18},{18,... | collective-permute-start | bytes 589832 | tf_op jit(solution)/shard_map/ppermute | solution.py:508
  13.8 33.6 %collective-permute-start.6 = (bf16[384,256]{1,0:T(8,128)(2,1)S(1)}, bf16[384,256]{1,0:T(8,128)(2,1)S(1)}, u32[]{:S(2)}, u32[]{:S(2)}) collective-permute-start(bf16[384,256]{1,0:T(8,128)(2,1)S(1)} %pad_maximum_fusion.6), channel_id=1, source_target_pairs={{0,4},{2,6},{4,0},{6,2},{8,12},{10,14},{12,8},{14,10},{16,20},{18,... | collective-permute-start | bytes 589832 | tf_op jit(solution)/shard_map/ppermute | solution.py:508
  24.3 23.1 %collective-permute-start.7 = (bf16[384,256]{1,0:T(8,128)(2,1)S(1)}, bf16[384,256]{1,0:T(8,128)(2,1)S(1)}, u32[]{:S(2)}, u32[]{:S(2)}) collective-permute-start(bf16[384,256]{1,0:T(8,128)(2,1)S(1)} %pad_maximum_fusion.7), channel_id=1, source_target_pairs={{0,6},{2,4},{4,2},{6,0},{8,14},{10,12},{12,10},{14,8},{16,22},{18,... | collective-permute-start | bytes 589832 | tf_op jit(solution)/shard_map/ppermute | solution.py:508
  38.9 11.7 %collective-permute-start.20 = (bf16[256,256]{1,0:T(8,128)(2,1)S(1)}, bf16[256,256]{1,0:T(8,128)(2,1)S(1)}, u32[]{:S(2)}, u32[]{:S(2)}) collective-permute-start(bf16[256,256]{1,0:T(8,128)(2,1)S(1)} %pad_maximum_fusion.8), channel_id=1, source_target_pairs={{0,2},{2,0},{4,6},{6,4},{8,10},{10,8},{12,14},{14,12},{16,18},{18,... | collective-permute-start | bytes 393224 | tf_op jit(solution)/shard_map/ppermute | solution.py:508
  38.9 11.7 %collective-permute-start.21 = (bf16[256,256]{1,0:T(8,128)(2,1)S(1)}, bf16[256,256]{1,0:T(8,128)(2,1)S(1)}, u32[]{:S(2)}, u32[]{:S(2)}) collective-permute-start(bf16[256,256]{1,0:T(8,128)(2,1)S(1)} %pad_maximum_fusion.9), channel_id=1, source_target_pairs={{0,4},{2,6},{4,0},{6,2},{8,12},{10,14},{12,8},{14,10},{16,20},{18,... | collective-permute-start | bytes 393224 | tf_op jit(solution)/shard_map/ppermute | solution.py:508
  45.5 77.9 %collective-permute-start.4 = (bf16[1024,1152]{1,0:T(8,128)(2,1)S(1)}, bf16[1024,1152]{1,0:T(8,128)(2,1)}, u32[]{:S(2)}, u32[]{:S(2)}) collective-permute-start(bf16[1024,1152]{1,0:T(8,128)(2,1)S(1)} %pad_maximum_fusion.refs_0_.refs_2_), channel_id=1, source_target_pairs={{0,1},{1,0},{2,3},{3,2},{4,5},{5,4},{6,7},{7,6},{8,9},{9,8},{10,11... | collective-permute-start | bytes 7077896 | tf_op jit(solution)/shard_map/ppermute | solution.py:516
  47.4 14.5 %collective-permute-start.8 = (bf16[1024,256]{1,0:T(8,128)(2,1)S(1)}, bf16[1024,256]{1,0:T(8,128)(2,1)S(1)}, u32[]{:S(2)}, u32[]{:S(2)}) collective-permute-start(bf16[1024,256]{1,0:T(8,128)(2,1)S(1)} %slice_dynamic-update-slice_fusion.refs_2_), channel_id=1, source_target_pairs={{0,8},{2,10},{4,12},{6,14},{8,16},{10,18},{12,20},{14,22},{16,24},... | collective-permute-start | bytes 1572872 | tf_op jit(solution)/shard_map/ppermute | solution.py:513
  49.0 12.9 %collective-permute-start.22 = (bf16[256,256]{1,0:T(8,128)(2,1)S(1)}, bf16[256,256]{1,0:T(8,128)(2,1)S(1)}, u32[]{:S(2)}, u32[]{:S(2)}) collective-permute-start(bf16[256,256]{1,0:T(8,128)(2,1)S(1)} %pad_maximum_fusion.10), channel_id=1, source_target_pairs={{0,6},{2,4},{4,2},{6,0},{8,14},{10,12},{12,10},{14,8},{16,22},{18,... | collective-permute-start | bytes 393224 | tf_op jit(solution)/shard_map/ppermute | solution.py:508
  61.9 16.7 %collective-permute-start.9 = (bf16[1024,256]{1,0:T(8,128)(2,1)S(1)}, bf16[1024,256]{1,0:T(8,128)(2,1)}, u32[]{:S(2)}, u32[]{:S(2)}) collective-permute-start(bf16[1024,256]{1,0:T(8,128)(2,1)S(1)} %collective-permute-done.8.refs_3_), channel_id=1, source_target_pairs={{0,8},{2,10},{4,12},{6,14},{8,16},{10,18},{12,20},{14,22},{16,24},... | collective-permute-start | bytes 1572872 | tf_op jit(solution)/shard_map/ppermute | solution.py:513
  61.9 22.3 %collective-permute-start.29 = (bf16[512,256]{1,0:T(8,128)(2,1)S(1)}, bf16[512,256]{1,0:T(8,128)(2,1)}, u32[]{:S(2)}, u32[]{:S(2)}) collective-permute-start(bf16[512,256]{1,0:T(8,128)(2,1)S(1)} %pad_maximum_fusion.4.refs_6_), channel_id=1, source_target_pairs={{0,8},{2,10},{4,12},{6,14},{8,16},{10,18},{12,20},{14,22},{16,24},... | collective-permute-start | bytes 786440 | tf_op jit(solution)/shard_map/ppermute | solution.py:513
  63.3 26.4 %collective-permute-start.23 = (bf16[512,256]{1,0:T(8,128)(2,1)S(1)}, bf16[512,256]{1,0:T(8,128)(2,1)S(1)}, u32[]{:S(2)}, u32[]{:S(2)}) collective-permute-start(bf16[512,256]{1,0:T(8,128)(2,1)S(1)} %pad_maximum_fusion.2.refs_2_), channel_id=1, source_target_pairs={{0,8},{2,10},{4,12},{6,14},{8,16},{10,18},{12,20},{14,22},{16,24},... | collective-permute-start | bytes 786440 | tf_op jit(solution)/shard_map/ppermute | solution.py:513
  65.0 30.4 %collective-permute-start.26 = (bf16[512,256]{1,0:T(8,128)(2,1)S(1)}, bf16[512,256]{1,0:T(8,128)(2,1)}, u32[]{:S(2)}, u32[]{:S(2)}) collective-permute-start(bf16[512,256]{1,0:T(8,128)(2,1)S(1)} %pad_maximum_fusion.3.refs_2_), channel_id=1, source_target_pairs={{0,8},{2,10},{4,12},{6,14},{8,16},{10,18},{12,20},{14,22},{16,24},... | collective-permute-start | bytes 786440 | tf_op jit(solution)/shard_map/ppermute | solution.py:513
  78.6 44.8 %collective-permute-start.10 = (bf16[1024,256]{1,0:T(8,128)(2,1)}, bf16[1024,256]{1,0:T(8,128)(2,1)}, u32[]{:S(2)}, u32[]{:S(2)}) collective-permute-start(bf16[1024,256]{1,0:T(8,128)(2,1)} %collective-permute-done.9.refs_4_), channel_id=1, source_target_pairs={{0,8},{2,10},{4,12},{6,14},{8,16},{10,18},{12,20},{14,22},{16,24},... | collective-permute-start | bytes 1572872 | tf_op jit(solution)/shard_map/ppermute | solution.py:513
  84.2 28.0 %collective-permute-start.30 = (bf16[512,256]{1,0:T(8,128)(2,1)}, bf16[512,256]{1,0:T(8,128)(2,1)S(1)}, u32[]{:S(2)}, u32[]{:S(2)}) collective-permute-start(bf16[512,256]{1,0:T(8,128)(2,1)} %collective-permute-done.29.refs_7_), channel_id=1, source_target_pairs={{0,8},{2,10},{4,12},{6,14},{8,16},{10,18},{12,20},{14,22},{16,24},... | collective-permute-start | bytes 786440 | tf_op jit(solution)/shard_map/ppermute | solution.py:513
  89.7 28.1 %collective-permute-start.24 = (bf16[512,256]{1,0:T(8,128)(2,1)S(1)}, bf16[512,256]{1,0:T(8,128)(2,1)S(1)}, u32[]{:S(2)}, u32[]{:S(2)}) collective-permute-start(bf16[512,256]{1,0:T(8,128)(2,1)S(1)} %collective-permute-done.23.refs_3_), channel_id=1, source_target_pairs={{0,8},{2,10},{4,12},{6,14},{8,16},{10,18},{12,20},{14,22},{16,24},... | collective-permute-start | bytes 786440 | tf_op jit(solution)/shard_map/ppermute | solution.py:513
  95.4 28.0 %collective-permute-start.27 = (bf16[512,256]{1,0:T(8,128)(2,1)}, bf16[512,256]{1,0:T(8,128)(2,1)S(1)}, u32[]{:S(2)}, u32[]{:S(2)}) collective-permute-start(bf16[512,256]{1,0:T(8,128)(2,1)} %collective-permute-done.26.refs_3_), channel_id=1, source_target_pairs={{0,8},{2,10},{4,12},{6,14},{8,16},{10,18},{12,20},{14,22},{16,24},... | collective-permute-start | bytes 786440 | tf_op jit(solution)/shard_map/ppermute | solution.py:513
  112.2 27.2 %collective-permute-start.31 = (bf16[512,256]{1,0:T(8,128)(2,1)S(1)}, bf16[512,256]{1,0:T(8,128)(2,1)S(1)}, u32[]{:S(2)}, u32[]{:S(2)}) collective-permute-start(bf16[512,256]{1,0:T(8,128)(2,1)S(1)} %collective-permute-done.30.refs_8_), channel_id=1, source_target_pairs={{0,8},{2,10},{4,12},{6,14},{8,16},{10,18},{12,20},{14,22},{16,24},... | collective-permute-start | bytes 786440 | tf_op jit(solution)/shard_map/ppermute | solution.py:513
  117.8 43.1 %collective-permute-start.25 = (bf16[512,256]{1,0:T(8,128)(2,1)S(1)}, bf16[512,256]{1,0:T(8,128)(2,1)S(1)}, u32[]{:S(2)}, u32[]{:S(2)}) collective-permute-start(bf16[512,256]{1,0:T(8,128)(2,1)S(1)} %collective-permute-done.24.refs_4_), channel_id=1, source_target_pairs={{0,8},{2,10},{4,12},{6,14},{8,16},{10,18},{12,20},{14,22},{16,24},... | collective-permute-start | bytes 786440 | tf_op jit(solution)/shard_map/ppermute | solution.py:513
  123.4 15.9 %collective-permute-start.28 = (bf16[512,256]{1,0:T(8,128)(2,1)S(1)}, bf16[512,256]{1,0:T(8,128)(2,1)S(1)}, u32[]{:S(2)}, u32[]{:S(2)}) collective-permute-start(bf16[512,256]{1,0:T(8,128)(2,1)S(1)} %collective-permute-done.27.refs_4_), channel_id=1, source_target_pairs={{0,8},{2,10},{4,12},{6,14},{8,16},{10,18},{12,20},{14,22},{16,24},... | collective-permute-start | bytes 786440 | tf_op jit(solution)/shard_map/ppermute | solution.py:513
  129.8 24.8 %collective-permute-start.11 = (bf16[16,256]{1,0:T(8,128)(2,1)S(1)}, bf16[16,256]{1,0:T(8,128)(2,1)S(1)}, u32[]{:S(2)}, u32[]{:S(2)}) collective-permute-start(bf16[16,256]{1,0:T(8,128)(2,1)S(1)} %get-tuple-element.28), channel_id=1, source_target_pairs={{0,8},{2,10},{4,12},{6,14},{8,16},{10,18},{12,20},{14,22},{16,24},... | collective-permute-start | bytes 24584 | tf_op jit(solution)/shard_map/ppermute | solution.py:513
  131.2 24.3 %collective-permute-start.12 = (bf16[16,256]{1,0:T(8,128)(2,1)S(1)}, bf16[16,256]{1,0:T(8,128)(2,1)S(1)}, u32[]{:S(2)}, u32[]{:S(2)}) collective-permute-start(bf16[16,256]{1,0:T(8,128)(2,1)S(1)} %get-tuple-element.29), channel_id=1, source_target_pairs={{8,0},{10,2},{12,4},{14,6},{16,8},{18,10},{20,12},{22,14},{24,16},... | collective-permute-start | bytes 24584 | tf_op jit(solution)/shard_map/ppermute | solution.py:513
  147.0 24.7 %collective-permute-start.32 = (bf16[272,256]{1,0:T(8,128)(2,1)S(1)}, bf16[272,256]{1,0:T(8,128)(2,1)S(1)}, u32[]{:S(2)}, u32[]{:S(2)}) collective-permute-start(bf16[272,256]{1,0:T(8,128)(2,1)S(1)} %get-tuple-element.42), channel_id=1, source_target_pairs={{0,8},{2,10},{4,12},{6,14},{8,16},{10,18},{12,20},{14,22},{16,24},... | collective-permute-start | bytes 417800 | tf_op jit(solution)/shard_map/ppermute | solution.py:513
  149.7 23.5 %collective-permute-start.33 = (bf16[272,256]{1,0:T(8,128)(2,1)S(1)}, bf16[272,256]{1,0:T(8,128)(2,1)S(1)}, u32[]{:S(2)}, u32[]{:S(2)}) collective-permute-start(bf16[272,256]{1,0:T(8,128)(2,1)S(1)} %get-tuple-element.43), channel_id=1, source_target_pairs={{0,16},{2,18},{4,20},{6,22},{8,24},{10,26},{12,28},{14,30},{16,0},... | collective-permute-start | bytes 417800 | tf_op jit(solution)/shard_map/ppermute | solution.py:513
  154.6 18.6 %collective-permute-start.34 = (bf16[272,256]{1,0:T(8,128)(2,1)S(1)}, bf16[272,256]{1,0:T(8,128)(2,1)S(1)}, u32[]{:S(2)}, u32[]{:S(2)}) collective-permute-start(bf16[272,256]{1,0:T(8,128)(2,1)S(1)} %get-tuple-element.44), channel_id=1, source_target_pairs={{0,24},{2,26},{4,28},{6,30},{8,0},{10,2},{12,4},{14,6},{16,8},{18,... | collective-permute-start | bytes 417800 | tf_op jit(solution)/shard_map/ppermute | solution.py:513
  160.8 8.8 %collective-permute-start.13 = (f32[8,1024]{1,0:T(8,128)S(1)}, f32[8,1024]{1,0:T(8,128)S(1)}, u32[]{:S(2)}, u32[]{:S(2)}) collective-permute-start(f32[8,1024]{1,0:T(8,128)S(1)} %get-tuple-element.31), channel_id=1, source_target_pairs={{0,1},{1,0},{2,3},{3,2},{4,5},{5,4},{6,7},{7,6},{8,9},{9,8},{10,11... | collective-permute-start | bytes 98312 | tf_op jit(solution)/shard_map/ppermute | solution.py:516
  169.7 12.8 %collective-permute-start.14 = (f32[8,1024]{1,0:T(8,128)S(1)}, f32[8,1024]{1,0:T(8,128)S(1)}, u32[]{:S(2)}, u32[]{:S(2)}) collective-permute-start(f32[8,1024]{1,0:T(8,128)S(1)} %add.224.refs_0_), channel_id=1, source_target_pairs={{0,2},{2,0},{4,6},{6,4},{8,10},{10,8},{12,14},{14,12},{16,18},{18,... | collective-permute-start | bytes 98312 | tf_op jit(solution)/shard_map/ppermute | solution.py:508
  171.2 13.1 %collective-permute-start.15 = (f32[8,1024]{1,0:T(8,128)S(1)}, f32[8,1024]{1,0:T(8,128)S(1)}, u32[]{:S(2)}, u32[]{:S(2)}) collective-permute-start(f32[8,1024]{1,0:T(8,128)S(1)} %add.224.refs_0_), channel_id=1, source_target_pairs={{0,4},{2,6},{4,0},{6,2},{8,12},{10,14},{12,8},{14,10},{16,20},{18,... | collective-permute-start | bytes 98312 | tf_op jit(solution)/shard_map/ppermute | solution.py:508
  171.7 12.6 %collective-permute-start.16 = (f32[8,1024]{1,0:T(8,128)S(1)}, f32[8,1024]{1,0:T(8,128)S(1)}, u32[]{:S(2)}, u32[]{:S(2)}) collective-permute-start(f32[8,1024]{1,0:T(8,128)S(1)} %add.224.refs_0_), channel_id=1, source_target_pairs={{0,6},{2,4},{4,2},{6,0},{8,14},{10,12},{12,10},{14,8},{16,22},{18,... | collective-permute-start | bytes 98312 | tf_op jit(solution)/shard_map/ppermute | solution.py:508
  187.2 7.9 %collective-permute-start.18 = (bf16[256,256]{1,0:T(8,128)(2,1)S(1)}, bf16[256,256]{1,0:T(8,128)(2,1)S(1)}, u32[]{:S(2)}, u32[]{:S(2)}) collective-permute-start(bf16[256,256]{1,0:T(8,128)(2,1)S(1)} %get-tuple-element.34), channel_id=1, source_target_pairs={{0,4},{2,6},{4,0},{6,2},{8,12},{10,14},{12,8},{14,10},{16,20},{18,... | collective-permute-start | bytes 393224 | tf_op jit(solution)/shard_map/ppermute | solution.py:508
  (21 other events, 349.3 us)
where the time goes:
time: 200 us; the launch traced here: 199 us
  waiting for transfers between devices  93.5 us (47%)
  starting transfers between devices  43.9 us (22%)
  Pallas kernels  42.9 us (21%)
  other arithmetic  8.92 us (4%)
  local copies, waits for them, and re-layouts  7.07 us (4%)
  matrix products  2.63 us (1%)
    ppermute x17, waiting for transfers between devices, along(): return lax.ppermute(x, 'sp', pairs)  64.6 us
    ppermute x18, waiting for transfers between devices, in_plane(): return lax.ppermute(x, 'sp', pairs)  27 us
    ppermute x18, starting transfers between devices, in_plane(): return lax.ppermute(x, 'sp', pairs)  25 us
    ppermute x17, starting transfers between devices, along(): return lax.ppermute(x, 'sp', pairs)  18.1 us
    pallas_call x1, Pallas kernels, shards(): call(functools.partial(local_kernel, (group, blocks, rows, n_parts, n_pie...  8.71 us
    pallas_call x1, Pallas kernels, shards(): call(functools.partial(states_kernel, (group, blocks, rows, n_parts, n_pi...  7.61 us
    pallas_call x1, Pallas kernels, shards(): call(functools.partial(finish_kernel, (group, len(states), ringed, halves...  7.11 us
    pallas_call x1, Pallas kernels, shards(): call(functools.partial(gates_kernel, (group, n_parts, extra_at, key_scale...  6.62 us
  transfers between devices with their start and end apart: 39, of which 16 were waited for; matrix products, arithmetic and copies ran while one was open for 7% of the time, Pallas kernels for 22%

commit v1 on v0

--- a/solution.py
+++ b/solution.py
@@ -76,26 +76,22 @@
     return made
 
 
-def fetch_parts(tab, group, parts, held, sems):
-    count, wide = held.shape[2:]
+def fetch_parts(tab, parts, held, sems):
+    group, wide = held.shape[1], held.shape[3]
     copies = []
-    for block in range(group):
-        rows = pl.ds(pl.multiple_of(tab[2 * group + block] * count, count), count)
-        for place, part in enumerate(parts):
-            copies.append(
-                (part.at[rows, pl.ds(0, wide)], held.at[place, block], sems.at[block * len(parts) + place])
-            )
-    made = fetch(copies)
-    return [made[block * len(parts) : (block + 1) * len(parts)] for block in range(group)]
-
-
-def fetch_weights(tab, group, blocks, rows, pieces, scratches, sems):
+    for spot, part in enumerate(parts):
+        copies.append((part.at[:, pl.ds(0, wide)], held.at[spot // group, tab[spot % group]], sems.at[spot]))
+    return fetch(copies)
+
+
+def fetch_weights(tab, group, blocks, rows, pieces, scratches, sems, by_slot=False):
     kinds = len(scratches)
     first = 3 * group + 5
     per = pieces[0].shape[0] // (rows * kinds)
     copies = []
     for block in range(blocks):
-        start = pl.multiple_of(tab[first + block], rows)
+        entry = block % per * group + block // per if by_slot else block
+        start = pl.multiple_of(tab[first + entry], rows)
         for kind, scratch in enumerate(scratches):
             at = (block % per * kinds + kind) * rows
             copies.append(
@@ -121,32 +117,31 @@
 
 def gates_kernel(dims, tab, *refs):
     group, n_parts, extra_at, key_scale = dims
-    parts = refs[:n_parts]
-    extra, gate_rows, gate_bias, rows_out, held, extra_in, rows_in, gates, extras, part_sems, sems = refs[n_parts:]
+    parts, extra = refs[:n_parts], refs[n_parts : n_parts + group]
+    gate_rows, gate_bias, rows_out, held, extra_in, rows_in, gates, extras, part_sems, sems = refs[n_parts + group :]
     core, head = tab[3 * group + 2], tab[3 * group + 4]
-    waits = fetch_parts(tab, group, parts, held, part_sems)
+    waits = fetch_parts(tab, parts, held, part_sems)
     count = held.shape[2]
     copies = [(gate_rows, rows_in, sems.at[group])]
-    for block in range(group):
-        rows = pl.ds(pl.multiple_of(tab[2 * group + block] * count, count), count)
-        copies.append((extra.at[rows, pl.ds(extra_at * 128, 128)], extra_in.at[block], sems.at[block]))
+    for slot, more in enumerate(extra):
+        copies.append((more.at[:, pl.ds(extra_at * 128, 128)], extra_in.at[tab[slot]], sems.at[slot]))
     rows_wait, *extra_waits = fetch(copies)
     line = lax.broadcasted_iota(jnp.int32, (2 * MEMORY_HEADS, 128), 0)
     column = lax.broadcasted_iota(jnp.int32, (2 * MEMORY_HEADS, 128), 1)
     select = (column % (2 * MEMORY_HEADS) == line) & (column < 6 * MEMORY_HEADS)
     select = jnp.where(select, 1.0, 0.0).astype(BF16)
     rows_wait.wait()
+    arrived(waits)
+    arrived(extra_waits)
     for block in range(group):
         here = slice(block * count, (block + 1) * count)
-        arrived(waits[block])
         pre = None
-        for place in range(n_parts):
+        for place in range(held.shape[0]):
             wide = held.shape[3]
-            start = 0 if n_parts == 1 else pl.multiple_of((core if place == 0 else 1 - core) * wide, wide)
+            start = 0 if held.shape[0] == 1 else pl.multiple_of((core if place == 0 else 1 - core) * wide, wide)
             term = dot_nt(rows_in[:, pl.ds(start, wide)], held[place, block])
             pre = term if pre is None else pre + term
         gates[:, here] = pre
-        extra_waits[block].wait()
         extras[:, here] = dot_nt(select, extra_in[block])
     width = gates.shape[1]
 
@@ -173,15 +168,17 @@
 
 def front_kernel(dims, tab, *refs):
     group, blocks, rows, n_parts, n_pieces = dims
-    parts, pieces = refs[:n_parts], refs[n_parts : n_parts + n_pieces]
-    glu_out, head_out, tail_out, held, value_w, gate_w, part_sems, sems = refs[n_parts + n_pieces :]
-    weight_waits = fetch_weights(tab, group, blocks, rows, pieces, (value_w, gate_w), sems)
-    waits = fetch_parts(tab, group, parts, held, part_sems)
+    parts, refs = refs[:n_parts], refs[n_parts:]
+    pieces, gate_pieces, refs = refs[:n_pieces], refs[n_pieces : 2 * n_pieces], refs[2 * n_pieces :]
+    glu_out, head_out, tail_out, held, value_w, gate_w, part_sems, sems = refs
+    weight_waits = fetch_weights(tab, group, blocks, rows, pieces, (value_w,), sems.at[pl.ds(0, 1)])
+    weight_waits += fetch_weights(tab, group, blocks, rows, gate_pieces, (gate_w,), sems.at[pl.ds(1, 1)])
+    waits = fetch_parts(tab, parts, held, part_sems)
     arrived(weight_waits)
+    arrived(waits)
     count = held.shape[2]
     for block in range(group):
-        arrived(waits[block])
-        have = [held[place, block] for place in range(n_parts)]
+        have = [held[place, block] for place in range(held.shape[0])]
         glu = (project(have, value_w) * jax.nn.sigmoid(project(have, gate_w))).astype(BF16)
         glu_out[block * count : (block + 1) * count, :] = glu
         if block == 0:
@@ -202,17 +199,17 @@
     key_wait = fetch_weights(tab, group, blocks, rows, key_pieces, (key_w,), sems.at[pl.ds(0, 1)])
     value_wait = fetch_weights(tab, group, blocks, rows, value_pieces, (value_w,), sems.at[pl.ds(1, 1)])
     table_wait = fetch([(table_in, table, sems.at[2])])
-    waits = fetch_parts(tab, group, parts, held, part_sems)
+    waits = fetch_parts(tab, parts, held, part_sems)
     arrived(key_wait)
     arrived(value_wait)
     arrived(table_wait)
+    arrived(waits)
     count = held.shape[2]
     columns = jnp.transpose(table[...])
     mats, sums = [None, None], [None, None]
     for block in range(group):
         here = slice(block * count, (block + 1) * count)
-        arrived(waits[block])
-        have = [held[place, block] for place in range(n_parts)]
+        have = [held[place, block] for place in range(held.shape[0])]
         keys = project(have, key_w).astype(BF16)
         key_out[here, :] = keys
         values = project(have, value_w).astype(BF16)
@@ -255,12 +252,13 @@
     keys_in, values_in, table_in = refs[n_parts + n_pieces : n_parts + n_pieces + 3]
     query_out, numer_f, numer_b, denom_out = refs[n_parts + n_pieces + 3 : n_parts + n_pieces + 7]
     held, query_w, keys, values, table, part_sems, sems = refs[n_parts + n_pieces + 7 :]
-    weight_wait = fetch_weights(tab, group, blocks, rows, pieces, (query_w,), sems.at[pl.ds(3, 1)])
-    waits = fetch_parts(tab, group, parts, held, part_sems)
+    weight_wait = fetch_weights(tab, group, blocks, rows, pieces, (query_w,), sems.at[pl.ds(3, 1)], True)
+    waits = fetch_parts(tab, parts, held, part_sems)
     others_wait = fetch(
         [(keys_in, keys, sems.at[0]), (values_in, values, sems.at[1]), (table_in, table, sems.at[2])]
     )
     arrived(weight_wait)
+    arrived(waits)
     length = keys.shape[0]
     count = length // group
     spot_t = lax.broadcasted_iota(jnp.int32, (count, count), 0)
@@ -269,8 +267,7 @@
     lane = lax.broadcasted_iota(jnp.int32, (count, 128), 1)
     for block in range(group):
         here = slice(block * count, (block + 1) * count)
-        arrived(waits[block])
-        queries = project([held[place, block] for place in range(n_parts)], query_w).astype(BF16)
+        queries = project([held[place, block] for place in range(held.shape[0])], query_w).astype(BF16)
         query_out[here, :] = queries
         if block == 0:
             arrived(others_wait)
@@ -418,8 +415,7 @@
     mats, vecs, bests = [], [], []
     for these in (ahead, back):
         mat, vec, best = incoming(these)
-        high = mat.astype(BF16)
-        mats.append((high, (mat - high.astype(F32)).astype(BF16)))
+        mats.append(mat.astype(BF16))
         vecs.append(vec)
         bests.append(best[:, 0:1])
     line = lax.broadcasted_iota(jnp.int32, (128, HEAD), 0)
@@ -443,9 +439,9 @@
         inverse = 1.0 / jnp.maximum(jnp.abs(denom), floor[here, :])
         left, right = stay[here, :] * inverse, carry[here, :] * inverse
         summed = None
-        for way, (high, low) in enumerate(mats):
+        for way, mat in enumerate(mats):
             term = left[:, way : way + 1] * numers[way, here, :].astype(F32)
-            term = term + right[:, way : way + 1] * (dot(queries, high) + dot(queries, low))
+            term = term + right[:, way : way + 1] * dot(queries, mat)
             summed = term if summed is None else summed + term
         scale = lax.rsqrt(jnp.mean(summed * summed, axis=1, keepdims=True) + EPS)
         result[here, :] = (summed * scale * gain[...]).astype(BF16)
@@ -550,9 +546,9 @@
     entries = (*sources, *targets, *inverse, quarter, 0, core, place, head, *offsets)
     tab = jnp.stack([jnp.asarray(x, jnp.int32) for x in entries])
 
-    got = split_weights([glu_value, glu_gate, key_weight], channels)
-    glu_piece = tall([x[: 2 * rows] for x in got])
-    key_piece = tall([x[2 * rows :] for x in got])
+    glu_piece = tall(split_weights([glu_value], channels))
+    gate_piece = tall(split_weights([glu_gate], channels))
+    key_piece = tall(split_weights([key_weight], HEAD))
     wide = tokens.astype(F32)
     squares = jnp.sum(wide * wide, axis=-1, keepdims=True)
     squares = squares + swap(squares) if paired else lax.psum(squares, "tp")
@@ -562,23 +558,28 @@
     extras = jnp.pad(jnp.concatenate(extras, 1), ((0, 0), (0, 128 - 3 * 2 * MEMORY_HEADS)))
     own_width = tokens.shape[1]
     payload = jnp.concatenate([normed, extras], 1)
-    payload = tall([in_plane(payload, slot) for slot in slots])
+    payloads = [in_plane(payload, slot) for slot in slots]
     if paired:
-        parts, extra_at = [payload, swap(payload)], own_width // 128
-        extra = payload
-        part_width = own_width
+        parts = payloads + [swap(x) for x in payloads]
+        extra, extra_at, part_width = payloads, own_width // 128, own_width
     else:
-        parts, extra_at = [lax.all_gather(payload[:, :own_width], "tp", axis=1, tiled=True)], 0
-        extra = payload[:, own_width:]
-        part_width = features
+        parts = [lax.all_gather(x[:, :own_width], "tp", axis=1, tiled=True) for x in payloads]
+        extra, extra_at, part_width = [x[:, own_width:] for x in payloads], 0, features
     glu_pieces = ring(glu_piece)
-    got = split_weights([value_weight, query_weight], HEAD)
-    value_piece, query_piece = [tall([x[m * rows : (m + 1) * rows] for x in got]) for m in range(2)]
+    gate_pieces = ring(gate_piece)
+    value_piece = tall(split_weights([value_weight], HEAD))
     conv_rows = tall([lax.dynamic_slice_in_dim(out_conv, at * channels, channels, 0) for at in sources])
     mem_rows = tall([lax.dynamic_slice_in_dim(out_mem, at * HEAD, HEAD, 0) for at in sources])
     key_pieces = ring(key_piece)
     value_pieces = ring(value_piece)
-    query_pieces = ring(query_piece)
+    query_rows = ring(query_weight)
+    query_cuts = []
+    for held_rows in query_rows:
+        query_cuts.append([lax.dynamic_slice_in_dim(held_rows, to * HEAD, HEAD, 1) for to in targets])
+    query_pieces = []
+    for slot in slots:
+        sent = [cut[slot] for cut in query_cuts]
+        query_pieces.append(in_plane(tall(sent), slot))
 
     def far(arrays):
         return [pl.BlockSpec(memory_space=pl.ANY) for _ in arrays]
@@ -610,12 +611,12 @@
     n_parts, n_pieces = len(parts), len(key_pieces)
     halves = 2 if paired else 1
     work = 2 * length * features * HEAD
-    held = [pltpu.VMEM((n_parts, group, count, part_width), BF16)]
-    part_sems = [dma(group * n_parts)]
+    held = [pltpu.VMEM((n_parts // group, group, count, part_width), BF16)]
+    part_sems = [dma(n_parts)]
     square = [pltpu.VMEM((features, HEAD), BF16)]
     table = call(
         functools.partial(gates_kernel, (group, n_parts, extra_at, key_scale)),
-        far(parts) + far([extra, gate_weight]) + [pl.BlockSpec(memory_space=pltpu.SMEM)],
+        far(parts) + far(extra) + far([gate_weight]) + [pl.BlockSpec(memory_space=pltpu.SMEM)],
         whole((8, length)),
         shape((8, length), F32),
         held
@@ -624,17 +625,17 @@
         + part_sems
         + [dma(group + 1)],
         work,
-    )(tab, *parts, extra, gate_weight.T, gate_bias)
+    )(tab, *parts, *extra, gate_weight.T, gate_bias)
 
     made = [shape((length, channels)), shape((HALO, channels)), shape((HALO, channels))]
     glu, glu_head, glu_tail = call(
         functools.partial(front_kernel, (group, blocks, rows, n_parts, n_pieces)),
-        far(parts) + far(glu_pieces),
+        far(parts) + far(glu_pieces) + far(gate_pieces),
         wholes(made),
         made,
         held + [pltpu.VMEM((features, channels), BF16)] * 2 + part_sems + [dma(2)],
         2 * work,
-    )(tab, *parts, *glu_pieces)
+    )(tab, *parts, *glu_pieces, *gate_pieces)
 
     glu_before = along(glu_tail, 1)
     glu_after = along(glu_head, -1)
@@ -682,7 +683,7 @@
     tall_head = [pltpu.VMEM((length, HEAD), BF16)]
     made = [shape((length, HEAD))] * 3 + [shape((length, 128), F32)]
     locals_made = call(
-        functools.partial(local_kernel, (group, blocks, rows, n_parts, n_pieces, key_scale)),
+        functools.partial(local_kernel, (group, blocks, rows, n_parts, len(query_pieces), key_scale)),
         far(parts) + far(query_pieces) + far([keys, values, table]),
         wholes(made),
         made,
@@ -705,7 +706,7 @@
     )(tab, *locals_made, table, *states, mem_gain[None, :])
     memories = [in_plane(memory, slot) for slot, memory in enumerate(memories)]
 
-    partial = dot(jnp.concatenate(acts, 1), conv_rows)
+    partial = lax.optimization_barrier(dot(jnp.concatenate(acts, 1), conv_rows))
     result = (partial + dot(jnp.concatenate(memories, 1), mem_rows)).astype(BF16)
     if paired:
         half = count // 2

time: 200 us -> 188 us (0.940)
  waiting for transfers between devices: 93.5 us -> 65.3 us
  local copies, waits for them, and re-layouts: 7.07 us -> 21.6 us
  starting transfers between devices: 43.9 us -> 53.8 us
  Pallas kernels: 42.9 us -> 37.7 us
  other arithmetic: 8.92 us -> 5.44 us
    ppermute x18 -> x27, waiting for transfers between devices: 27 us -> 6.52 us  [in_plane(): return lax.ppermute(x, 'sp', pairs)]
    ppermute x18 -> x27, starting transfers between devices: 25 us -> 33.9 us  [in_plane(): return lax.ppermute(x, 'sp', pairs)]
    ppermute x17 -> x20, waiting for transfers between devices: 64.6 us -> 56.9 us  [along(): return lax.ppermute(x, 'sp', pairs)]
    unnamed x32 -> x76, local copies, waits for them, and re-layouts: 1.11 us -> 8.66 us
    dynamic_slice x0 -> x4, local copies, waits for them, and re-layouts: none -> 3.59 us  [shards(): lax.dynamic_slice_in_dim(held_rows, to * HEAD, HEAD, 1)]
    concatenate x10 -> x8, other arithmetic: 4.62 us -> 1.86 us  [tall(): return jnp.concatenate(x, axis=0) if len(x) > 1 else x[0]]
    pallas_call x1, Pallas kernels: 6.62 us -> 4.1 us  [shards(): call(functools.partial(gates_kernel, (group, n_parts, extra_at, key_scale...]
    dynamic_slice x1 -> x4, local copies, waits for them, and re-layouts: 1.74 us -> 3.83 us  [split_weights(): lax.dynamic_slice_in_dim(weight, to, width, 1)]
  transfers between devices with their start and end apart: 39 -> 54, of which waited for: 16 -> 20; matrix products, arithmetic and copies ran while one was open for 7% -> 9% of each run, Pallas kernels for 22% -> 20%
where the time goes in v1:
time: 188 us; the launch traced here: 187 us
  waiting for transfers between devices  65.3 us (35%)
  starting transfers between devices  53.8 us (29%)
  Pallas kernels  37.7 us (20%)
  local copies, waits for them, and re-layouts  21.6 us (11%)
  other arithmetic  5.44 us (3%)
  matrix products  2.51 us (1%)
    ppermute x20, waiting for transfers between devices, along(): return lax.ppermute(x, 'sp', pairs)  56.9 us
    ppermute x27, starting transfers between devices, in_plane(): return lax.ppermute(x, 'sp', pairs)  33.9 us
    ppermute x20, starting transfers between devices, along(): return lax.ppermute(x, 'sp', pairs)  18.6 us
    unnamed x76, local copies, waits for them, and re-layouts  8.66 us
    pallas_call x1, Pallas kernels, shards(): call(functools.partial(states_kernel, (group, blocks, rows, n_parts, n_pi...  7.08 us
    pallas_call x1, Pallas kernels, shards(): call(functools.partial(finish_kernel, (group, len(states), ringed, halves...  7.03 us
    pallas_call x1, Pallas kernels, shards(): call(functools.partial(local_kernel, (group, blocks, rows, n_parts, len(q...  6.64 us
    ppermute x27, waiting for transfers between devices, in_plane(): return lax.ppermute(x, 'sp', pairs)  6.52 us
  transfers between devices with their start and end apart: 54, of which 20 were waited for; matrix products, arithmetic and copies ran while one was open for 9% of the time, Pallas kernels for 20%

profile of v1, /device:TPU:0, one launch (start us, length us, event | category | flops | bytes accessed | tf_op | source)
XLA Modules:
  0.0 187.0 jit_solution(1331663612900745546)
XLA Ops:
  2.8 2.6 %collective-permute-start.14 = (bf16[128,256]{1,0:T(8,128)(2,1)S(1)}, bf16[128,256]{1,0:T(8,128)(2,1)S(1)}, u32[]{:S(2)}, u32[]{:S(2)}) collective-permute-start(bf16[128,256]{1,0:T(8,128)(2,1)S(1)} %get-tuple-element.82), channel_id=1, source_target_pairs={{0,2},{2,0},{4,6},{6,4},{8,10},{10,8},{12,14},{14,12},{16,18},{18,... | collective-permute-start | bytes 196616 | tf_op jit(solution)/shard_map/ppermute | solution.py:504
  13.2 2.0 %collective-permute-start.42 = (bf16[128,256]{1,0:T(8,128)(2,1)S(1)}, bf16[128,256]{1,0:T(8,128)(2,1)S(1)}, u32[]{:S(2)}, u32[]{:S(2)}) collective-permute-start(bf16[128,256]{1,0:T(8,128)(2,1)S(1)} %get-tuple-element.60), channel_id=1, source_target_pairs={{0,4},{2,6},{4,0},{6,2},{8,12},{10,14},{12,8},{14,10},{16,20},{18,... | collective-permute-start | bytes 196616 | tf_op jit(solution)/shard_map/ppermute | solution.py:504
  15.3 1.9 %collective-permute-start.35 = (bf16[128,256]{1,0:T(8,128)(2,1)S(1)}, bf16[128,256]{1,0:T(8,128)(2,1)S(1)}, u32[]{:S(2)}, u32[]{:S(2)}) collective-permute-start(bf16[128,256]{1,0:T(8,128)(2,1)S(1)} %get-tuple-element.62), channel_id=1, source_target_pairs={{0,2},{2,0},{4,6},{6,4},{8,10},{10,8},{12,14},{14,12},{16,18},{18,... | collective-permute-start | bytes 196616 | tf_op jit(solution)/shard_map/ppermute | solution.py:504
  18.0 2.3 %collective-permute-start.37 = (bf16[128,256]{1,0:T(8,128)(2,1)S(1)}, bf16[128,256]{1,0:T(8,128)(2,1)S(1)}, u32[]{:S(2)}, u32[]{:S(2)}) collective-permute-start(bf16[128,256]{1,0:T(8,128)(2,1)S(1)} %get-tuple-element.63), channel_id=1, source_target_pairs={{0,6},{2,4},{4,2},{6,0},{8,14},{10,12},{12,10},{14,8},{16,22},{18,... | collective-permute-start | bytes 196616 | tf_op jit(solution)/shard_map/ppermute | solution.py:504
  25.1 2.1 %collective-permute-start.10 = (bf16[128,256]{1,0:T(8,128)(2,1)S(1)}, bf16[128,256]{1,0:T(8,128)(2,1)S(1)}, u32[]{:S(2)}, u32[]{:S(2)}) collective-permute-start(bf16[128,256]{1,0:T(8,128)(2,1)S(1)} %get-tuple-element.87), channel_id=1, source_target_pairs={{0,6},{2,4},{4,2},{6,0},{8,14},{10,12},{12,10},{14,8},{16,22},{18,... | collective-permute-start | bytes 196616 | tf_op jit(solution)/shard_map/ppermute | solution.py:504
  33.9 4.2 %collective-permute-done.44.refs_13_ = bf16[512,256]{1,0:T(8,128)(2,1)S(1)} collective-permute-done((bf16[512,256]{1,0:T(8,128)(2,1)S(1)}, bf16[512,256]{1,0:T(8,128)(2,1)S(1)}, u32[]{:S(2)}, u32[]{:S(2)}) %collective-permute-start.44) | collective-permute-done | bytes 262176 | tf_op jit(solution)/shard_map/ppermute | solution.py:509
  38.4 5.3 %collective-permute-done.38.refs_9_ = bf16[512,256]{1,0:T(8,128)(2,1)S(1)} collective-permute-done((bf16[512,256]{1,0:T(8,128)(2,1)S(1)}, bf16[512,256]{1,0:T(8,128)(2,1)S(1)}, u32[]{:S(2)}, u32[]{:S(2)}) %collective-permute-start.38) | collective-permute-done | bytes 262176 | tf_op jit(solution)/shard_map/ppermute | solution.py:509
  44.9 4.5 %collective-permute-done.17.refs_13_ = bf16[512,256]{1,0:T(8,128)(2,1)S(1)} collective-permute-done((bf16[512,256]{1,0:T(8,128)(2,1)S(1)}, bf16[512,256]{1,0:T(8,128)(2,1)S(1)}, u32[]{:S(2)}, u32[]{:S(2)}) %collective-permute-start.17) | collective-permute-done | bytes 262176 | tf_op jit(solution)/shard_map/ppermute | solution.py:509
  50.5 4.5 %collective-permute-done.11.refs_9_ = bf16[512,256]{1,0:T(8,128)(2,1)S(1)} collective-permute-done((bf16[512,256]{1,0:T(8,128)(2,1)S(1)}, bf16[512,256]{1,0:T(8,128)(2,1)S(1)}, u32[]{:S(2)}, u32[]{:S(2)}) %collective-permute-start.11) | collective-permute-done | bytes 262176 | tf_op jit(solution)/shard_map/ppermute | solution.py:509
  55.3 5.4 %collective-permute-done.30 = bf16[128,1024]{1,0:T(8,128)(2,1)} collective-permute-done((bf16[128,1024]{1,0:T(8,128)(2,1)S(1)}, bf16[128,1024]{1,0:T(8,128)(2,1)}, u32[]{:S(2)}, u32[]{:S(2)}) %collective-permute-start.30) | collective-permute-done | bytes 262176 | tf_op jit(solution)/shard_map/ppermute | solution.py:509
  60.7 5.5 %collective-permute-done.45.refs_14_ = bf16[512,256]{1,0:T(8,128)(2,1)S(1)} collective-permute-done((bf16[512,256]{1,0:T(8,128)(2,1)S(1)}, bf16[512,256]{1,0:T(8,128)(2,1)S(1)}, u32[]{:S(2)}, u32[]{:S(2)}) %collective-permute-start.45) | collective-permute-done | bytes 262176 | tf_op jit(solution)/shard_map/ppermute | solution.py:509
  67.6 2.2 %constant_dynamic-slice_fusion.31 = (bf16[256,2048]{1,0:T(8,128)(2,1)}, bf16[256,2048]{1,0:T(8,128)(2,1)}, bf16[256,2048]{1,0:T(8,128)(2,1)}, bf16[256,2048]{1,0:T(8,128)(2,1)}) fusion(bf16[1024,2048]{1,0:T(8,128)(2,1)S(1)} %copy-done.24, s32[]{:T(128)S(6)} %select_n.165, s32[]{:T(128)S(6)} %select_n.166, s32[]{:T(128)S(6)} %select_n.168, s32[]{:T(128)S(6)} %select_n.167), kind=kLoop, calls=%fused_computation.83 | loop fusion | bytes 8388624 | tf_op jit(solution)/shard_map/dynamic_slice | solution.py:571
  71.1 4.0 %collective-permute-done.18.refs_14_ = bf16[512,256]{1,0:T(8,128)(2,1)S(1)} collective-permute-done((bf16[512,256]{1,0:T(8,128)(2,1)S(1)}, bf16[512,256]{1,0:T(8,128)(2,1)S(1)}, u32[]{:S(2)}, u32[]{:S(2)}) %collective-permute-start.18) | collective-permute-done | bytes 262176 | tf_op jit(solution)/shard_map/ppermute | solution.py:509
  75.9 2.2 %constant_dynamic-slice_fusion.3 = (bf16[256,2048]{1,0:T(8,128)(2,1)}, bf16[256,2048]{1,0:T(8,128)(2,1)}, bf16[256,2048]{1,0:T(8,128)(2,1)}, bf16[256,2048]{1,0:T(8,128)(2,1)}) fusion(bf16[1024,2048]{1,0:T(8,128)(2,1)S(1)} %copy-done.25, s32[]{:T(128)S(6)} %select_n.165, s32[]{:T(128)S(6)} %select_n.166, s32[]{:T(128)S(6)} %select_n.168, s32[]{:T(128)S(6)} %select_n.167), kind=kLoop, calls=%fused_computation.55 | loop fusion | bytes 8388624 | tf_op jit(solution)/shard_map/dynamic_slice | solution.py:572
  78.1 5.2 %collective-permute-done.12.refs_10_ = bf16[512,256]{1,0:T(8,128)(2,1)S(1)} collective-permute-done((bf16[512,256]{1,0:T(8,128)(2,1)S(1)}, bf16[512,256]{1,0:T(8,128)(2,1)S(1)}, u32[]{:S(2)}, u32[]{:S(2)}) %collective-permute-start.12) | collective-permute-done | bytes 262176 | tf_op jit(solution)/shard_map/ppermute | solution.py:509
  87.5 4.3 %collective-permute-done.31 = bf16[128,1024]{1,0:T(8,128)(2,1)} collective-permute-done((bf16[128,1024]{1,0:T(8,128)(2,1)}, bf16[128,1024]{1,0:T(8,128)(2,1)}, u32[]{:S(2)}, u32[]{:S(2)}) %collective-permute-start.31) | collective-permute-done | bytes 262176 | tf_op jit(solution)/shard_map/ppermute | solution.py:509
  94.5 4.2 %collective-permute-done.19.refs_15_ = bf16[512,256]{1,0:T(8,128)(2,1)S(1)} collective-permute-done((bf16[512,256]{1,0:T(8,128)(2,1)}, bf16[512,256]{1,0:T(8,128)(2,1)S(1)}, u32[]{:S(2)}, u32[]{:S(2)}) %collective-permute-start.19) | collective-permute-done | bytes 262176 | tf_op jit(solution)/shard_map/ppermute | solution.py:509
  98.7 5.6 %collective-permute-done.13.refs_11_ = bf16[512,256]{1,0:T(8,128)(2,1)S(1)} collective-permute-done((bf16[512,256]{1,0:T(8,128)(2,1)}, bf16[512,256]{1,0:T(8,128)(2,1)S(1)}, u32[]{:S(2)}, u32[]{:S(2)}) %collective-permute-start.13) | collective-permute-done | bytes 262176 | tf_op jit(solution)/shard_map/ppermute | solution.py:509
  110.3 6.3 %shard_map.154 = (bf16[1024,256]{1,0:T(8,128)(2,1)S(1)}, bf16[16,256]{1,0:T(8,128)(2,1)S(1)}, bf16[16,256]{1,0:T(8,128)(2,1)S(1)}) custom-call(s32[33]{0:T(128)S(1)} %stack.104.tab, bf16[256,1152]{1,0:T(8,128)(2,1)S(1)} %fusion.20.refs_0_.refs_8_, bf16[256,1152]{1,0:T(8,128)(2,1)S(1)} %collective-permute-done.1.refs_1_.refs_9_, ...), custom_call_target="tpu_custom_call" | custom-call | flops 2147483648 | bytes 4194304 | tf_op jit(solution)/shard_map/pallas_call | solution.py:631
  116.6 2.0 %collective-permute-start.20 = (bf16[16,256]{1,0:T(8,128)(2,1)S(1)}, bf16[16,256]{1,0:T(8,128)(2,1)S(1)}, u32[]{:S(2)}, u32[]{:S(2)}) collective-permute-start(bf16[16,256]{1,0:T(8,128)(2,1)S(1)} %get-tuple-element.28), channel_id=1, source_target_pairs={{0,8},{2,10},{4,12},{6,14},{8,16},{10,18},{12,20},{14,22},{16,24},... | collective-permute-start | bytes 24584 | tf_op jit(solution)/shard_map/ppermute | solution.py:509
  121.6 2.9 %collective-permute-done.21.after = bf16[16,256]{1,0:T(8,128)(2,1)S(1)} collective-permute-done((bf16[16,256]{1,0:T(8,128)(2,1)S(1)}, bf16[16,256]{1,0:T(8,128)(2,1)S(1)}, u32[]{:S(2)}, u32[]{:S(2)}) %collective-permute-start.21) | collective-permute-done | bytes 8224 | tf_op jit(solution)/shard_map/ppermute | solution.py:509
  124.5 5.3 %shard_map.155 = (f32[1024,256]{1,0:T(8,128)S(1)}, f32[8,1024]{1,0:T(8,128)S(1)}) custom-call(s32[33]{0:T(128)S(1)} %stack.104.tab, bf16[1024,256]{1,0:T(8,128)(2,1)S(1)} %get-tuple-element.27.glu, bf16[16,256]{1,0:T(8,128)(2,1)S(1)} %collective-permute-done.20.before, bf16[16,256]{1,0:T(8,128)(2,1)S(1)} %collective-permute-done.21.after, ...), custom_call_target="tpu_custom_call" | custom-call | flops 2147483648 | bytes 4194304 | tf_op jit(solution)/shard_map/pallas_call | solution.py:646
  129.9 4.1 %shard_map.157.refs_16_.refs_14_.refs_4_ = f32[8,1024]{1,0:T(8,128)S(1)} custom-call(s32[33]{0:T(128)S(1)} %stack.104.tab, bf16[256,1152]{1,0:T(8,128)(2,1)S(1)} %fusion.20.refs_0_.refs_8_, bf16[256,1152]{1,0:T(8,128)(2,1)S(1)} %collective-permute-done.1.refs_1_.refs_9_, bf16[256,1152]{1,0:T(8,128)(2,1)S(1)} %collective-permute-done.2.refs_2_.refs_10_, ...), custom_call_target="tpu_custom_call" | custom-call | flops 1073741824 | bytes 4194304 | tf_op jit(solution)/shard_map/pallas_call | solution.py:617
  134.1 2.4 %collective-permute-start.34 = (bf16[512,256]{1,0:T(8,128)(2,1)S(1)}, bf16[512,256]{1,0:T(8,128)(2,1)S(1)}, u32[]{:S(2)}, u32[]{:S(2)}) collective-permute-start(bf16[512,256]{1,0:T(8,128)(2,1)S(1)} %pad_maximum_fusion.5), channel_id=1, source_target_pairs={{0,6},{2,4},{4,2},{6,0},{8,14},{10,12},{12,10},{14,8},{16,22},{18,... | collective-permute-start | bytes 786440 | tf_op jit(solution)/shard_map/ppermute | solution.py:504
  137.2 7.1 %shard_map.158 = (bf16[1024,256]{1,0:T(8,128)(2,1)S(1)}, bf16[1024,256]{1,0:T(8,128)(2,1)S(1)}, bf16[272,256]{1,0:T(8,128)(2,1)S(1)}, bf16[272,256]{1,0:T(8,128)(2,1)S(1)}, bf16[272,256]{1,0:T(8,128)(2,1)S(1)}) custom-call(s32[33]{0:T(128)S(1)} %stack.104.tab, bf16[256,1152]{1,0:T(8,128)(2,1)S(1)} %fusion.20.refs_0_.refs_8_, ...), custom_call_target="tpu_custom_call" | custom-call | flops 2147483648 | bytes 4194304 | tf_op jit(solution)/shard_map/pallas_call | solution.py:670
  144.3 2.6 %collective-permute-start.47 = (bf16[272,256]{1,0:T(8,128)(2,1)S(1)}, bf16[272,256]{1,0:T(8,128)(2,1)S(1)}, u32[]{:S(2)}, u32[]{:S(2)}) collective-permute-start(bf16[272,256]{1,0:T(8,128)(2,1)S(1)} %get-tuple-element.42), channel_id=1, source_target_pairs={{0,8},{2,10},{4,12},{6,14},{8,16},{10,18},{12,20},{14,22},{16,24},... | collective-permute-start | bytes 417800 | tf_op jit(solution)/shard_map/ppermute | solution.py:509
  152.3 2.8 %collective-permute-start.49 = (bf16[272,256]{1,0:T(8,128)(2,1)S(1)}, bf16[272,256]{1,0:T(8,128)(2,1)S(1)}, u32[]{:S(2)}, u32[]{:S(2)}) collective-permute-start(bf16[272,256]{1,0:T(8,128)(2,1)S(1)} %get-tuple-element.44), channel_id=1, source_target_pairs={{0,24},{2,26},{4,28},{6,30},{8,0},{10,2},{12,4},{14,6},{16,8},{18,... | collective-permute-start | bytes 417800 | tf_op jit(solution)/shard_map/ppermute | solution.py:509
  159.9 6.6 %shard_map.159 = (bf16[1024,256]{1,0:T(8,128)(2,1)S(1)}, bf16[1024,256]{1,0:T(8,128)(2,1)S(1)}, bf16[1024,256]{1,0:T(8,128)(2,1)S(1)}, f32[1024,128]{1,0:T(8,128)S(1)}) custom-call(s32[33]{0:T(128)S(1)} %stack.104.tab, bf16[256,1152]{1,0:T(8,128)(2,1)S(1)} %fusion.20.refs_0_.refs_8_, bf16[256,1152]{1,0:T(8,128)(2,1)S(1)} %collective-permute-done.1.refs_1_.refs_9_, ...), custom_call_target="tpu_custom_call" | custom-call | flops 1073741824 | bytes 4194304 | tf_op jit(solution)/shard_map/pallas_call | solution.py:685
  166.6 7.0 %shard_map.160 = (bf16[256,256]{1,0:T(8,128)(2,1)S(1)}, bf16[256,256]{1,0:T(8,128)(2,1)S(1)}, bf16[256,256]{1,0:T(8,128)(2,1)S(1)}, bf16[256,256]{1,0:T(8,128)(2,1)S(1)}) custom-call(s32[33]{0:T(128)S(1)} %stack.104.tab, bf16[1024,256]{1,0:T(8,128)(2,1)S(1)} %get-tuple-element.38.refs_0_, bf16[1024,256]{1,0:T(8,128)(2,1)S(1)} %get-tuple-element.39.refs_1_, ...), custom_call_target="tpu_custom_call" | custom-call | flops 1073741824 | bytes 4194304 | tf_op jit(solution)/shard_map/pallas_call | solution.py:695
  173.6 1.8 collective-permute-start.50
  180.4 2.0 %collective-permute-done.52 = bf16[256,256]{1,0:T(8,128)(2,1)S(1)} collective-permute-done((bf16[256,256]{1,0:T(8,128)(2,1)S(1)}, bf16[256,256]{1,0:T(8,128)(2,1)S(1)}, u32[]{:S(2)}, u32[]{:S(2)}) %collective-permute-start.52) | collective-permute-done | bytes 131104 | tf_op jit(solution)/shard_map/ppermute | solution.py:504
  184.2 1.9 %collective-permute-done.53 = bf16[128,2048]{1,0:T(8,128)(2,1)S(1)} collective-permute-done((bf16[128,2048]{1,0:T(8,128)(2,1)S(1)}, bf16[128,2048]{1,0:T(8,128)(2,1)S(1)}, u32[]{:S(2)}, u32[]{:S(2)}) %collective-permute-start.53) | collective-permute-done | bytes 524320 | tf_op jit(solution)/shard_map/ppermute | solution.py:512
  (192 shorter events, 63.5 us)
Async XLA Ops:
  1.3 11.9 %collective-permute-start = (f32[256,1]{0,1:T(1,128)S(1)}, f32[256,1]{0,1:T(1,128)S(1)}, u32[]{:S(2)}, u32[]{:S(2)}) collective-permute-start(f32[256,1]{0,1:T(1,128)S(1)} %bitcast.34), channel_id=1, source_target_pairs={{0,1},{1,0},{2,3},{3,2},{4,5},{5,4},{6,7},{7,6},{8,9},{9,8},{10,11... | collective-permute-start | bytes 3080 | tf_op jit(solution)/shard_map/ppermute | solution.py:512
  2.8 17.6 %collective-permute-start.14 = (bf16[128,256]{1,0:T(8,128)(2,1)S(1)}, bf16[128,256]{1,0:T(8,128)(2,1)S(1)}, u32[]{:S(2)}, u32[]{:S(2)}) collective-permute-start(bf16[128,256]{1,0:T(8,128)(2,1)S(1)} %get-tuple-element.82), channel_id=1, source_target_pairs={{0,2},{2,0},{4,6},{6,4},{8,10},{10,8},{12,14},{14,12},{16,18},{18,... | collective-permute-start | bytes 196616 | tf_op jit(solution)/shard_map/ppermute | solution.py:504
  5.4 15.9 %collective-permute-start.16 = (bf16[128,256]{1,0:T(8,128)(2,1)S(1)}, bf16[128,256]{1,0:T(8,128)(2,1)S(1)}, u32[]{:S(2)}, u32[]{:S(2)}) collective-permute-start(bf16[128,256]{1,0:T(8,128)(2,1)S(1)} %get-tuple-element.83), channel_id=1, source_target_pairs={{0,6},{2,4},{4,2},{6,0},{8,14},{10,12},{12,10},{14,8},{16,22},{18,... | collective-permute-start | bytes 196616 | tf_op jit(solution)/shard_map/ppermute | solution.py:504
  21.3 11.8 %collective-permute-start.29 = (bf16[128,1024]{1,0:T(8,128)(2,1)}, bf16[128,1024]{1,0:T(8,128)(2,1)S(1)}, u32[]{:S(2)}, u32[]{:S(2)}) collective-permute-start(bf16[128,1024]{1,0:T(8,128)(2,1)} %param.23), channel_id=1, source_target_pairs={{0,8},{2,10},{4,12},{6,14},{8,16},{10,18},{12,20},{14,22},{16,24},... | collective-permute-start | bytes 786440 | tf_op jit(solution)/shard_map/ppermute | solution.py:509
  22.9 15.2 %collective-permute-start.44 = (bf16[512,256]{1,0:T(8,128)(2,1)S(1)}, bf16[512,256]{1,0:T(8,128)(2,1)S(1)}, u32[]{:S(2)}, u32[]{:S(2)}) collective-permute-start(bf16[512,256]{1,0:T(8,128)(2,1)S(1)} %pad_maximum_fusion.7.refs_12_), channel_id=1, source_target_pairs={{0,8},{2,10},{4,12},{6,14},{8,16},{10,18},{12,20},{14,22},{16,24},... | collective-permute-start | bytes 786440 | tf_op jit(solution)/shard_map/ppermute | solution.py:509
  28.8 14.9 %collective-permute-start.38 = (bf16[512,256]{1,0:T(8,128)(2,1)S(1)}, bf16[512,256]{1,0:T(8,128)(2,1)S(1)}, u32[]{:S(2)}, u32[]{:S(2)}) collective-permute-start(bf16[512,256]{1,0:T(8,128)(2,1)S(1)} %pad_maximum_fusion.6.refs_8_), channel_id=1, source_target_pairs={{0,8},{2,10},{4,12},{6,14},{8,16},{10,18},{12,20},{14,22},{16,24},... | collective-permute-start | bytes 786440 | tf_op jit(solution)/shard_map/ppermute | solution.py:509
  30.4 18.9 %collective-permute-start.17 = (bf16[512,256]{1,0:T(8,128)(2,1)S(1)}, bf16[512,256]{1,0:T(8,128)(2,1)S(1)}, u32[]{:S(2)}, u32[]{:S(2)}) collective-permute-start(bf16[512,256]{1,0:T(8,128)(2,1)S(1)} %pad_maximum_fusion.1.refs_12_), channel_id=1, source_target_pairs={{0,8},{2,10},{4,12},{6,14},{8,16},{10,18},{12,20},{14,22},{16,24},... | collective-permute-start | bytes 786440 | tf_op jit(solution)/shard_map/ppermute | solution.py:509
  31.9 23.1 %collective-permute-start.11 = (bf16[512,256]{1,0:T(8,128)(2,1)S(1)}, bf16[512,256]{1,0:T(8,128)(2,1)S(1)}, u32[]{:S(2)}, u32[]{:S(2)}) collective-permute-start(bf16[512,256]{1,0:T(8,128)(2,1)S(1)} %pad_maximum_fusion.refs_8_), channel_id=1, source_target_pairs={{0,8},{2,10},{4,12},{6,14},{8,16},{10,18},{12,20},{14,22},{16,24},... | collective-permute-start | bytes 786440 | tf_op jit(solution)/shard_map/ppermute | solution.py:509
  33.1 27.6 %collective-permute-start.30 = (bf16[128,1024]{1,0:T(8,128)(2,1)S(1)}, bf16[128,1024]{1,0:T(8,128)(2,1)}, u32[]{:S(2)}, u32[]{:S(2)}) collective-permute-start(bf16[128,1024]{1,0:T(8,128)(2,1)S(1)} %collective-permute-done.29), channel_id=1, source_target_pairs={{0,8},{2,10},{4,12},{6,14},{8,16},{10,18},{12,20},{14,22},{16,24},... | collective-permute-start | bytes 786440 | tf_op jit(solution)/shard_map/ppermute | solution.py:509
  38.1 28.1 %collective-permute-start.45 = (bf16[512,256]{1,0:T(8,128)(2,1)S(1)}, bf16[512,256]{1,0:T(8,128)(2,1)S(1)}, u32[]{:S(2)}, u32[]{:S(2)}) collective-permute-start(bf16[512,256]{1,0:T(8,128)(2,1)S(1)} %collective-permute-done.44.refs_13_), channel_id=1, source_target_pairs={{0,8},{2,10},{4,12},{6,14},{8,16},{10,18},{12,20},{14,22},{16,24},... | collective-permute-start | bytes 786440 | tf_op jit(solution)/shard_map/ppermute | solution.py:509
  43.7 41.1 %collective-permute-start.3 = (bf16[256,1152]{1,0:T(8,128)(2,1)S(1)}, bf16[256,1152]{1,0:T(8,128)(2,1)S(1)}, u32[]{:S(2)}, u32[]{:S(2)}) collective-permute-start(bf16[256,1152]{1,0:T(8,128)(2,1)S(1)} %fusion.20.refs_0_.refs_8_), channel_id=1, source_target_pairs={{0,6},{2,4},{4,2},{6,0},{8,14},{10,12},{12,10},{14,8},{16,22},{18,... | collective-permute-start | bytes 1769480 | tf_op jit(solution)/shard_map/ppermute | solution.py:504
  49.4 35.6 %collective-permute-start.2 = (bf16[256,1152]{1,0:T(8,128)(2,1)S(1)}, bf16[256,1152]{1,0:T(8,128)(2,1)S(1)}, u32[]{:S(2)}, u32[]{:S(2)}) collective-permute-start(bf16[256,1152]{1,0:T(8,128)(2,1)S(1)} %fusion.20.refs_0_.refs_8_), channel_id=1, source_target_pairs={{0,4},{2,6},{4,0},{6,2},{8,12},{10,14},{12,8},{14,10},{16,20},{18,... | collective-permute-start | bytes 1769480 | tf_op jit(solution)/shard_map/ppermute | solution.py:504
  55.0 30.4 %collective-permute-start.1 = (bf16[256,1152]{1,0:T(8,128)(2,1)S(1)}, bf16[256,1152]{1,0:T(8,128)(2,1)S(1)}, u32[]{:S(2)}, u32[]{:S(2)}) collective-permute-start(bf16[256,1152]{1,0:T(8,128)(2,1)S(1)} %fusion.20.refs_0_.refs_8_), channel_id=1, source_target_pairs={{0,2},{2,0},{4,6},{6,4},{8,10},{10,8},{12,14},{14,12},{16,18},{18,... | collective-permute-start | bytes 1769480 | tf_op jit(solution)/shard_map/ppermute | solution.py:504
  60.7 10.4 %collective-permute-start.39 = (bf16[512,256]{1,0:T(8,128)(2,1)S(1)}, bf16[512,256]{1,0:T(8,128)(2,1)}, u32[]{:S(2)}, u32[]{:S(2)}) collective-permute-start(bf16[512,256]{1,0:T(8,128)(2,1)S(1)} %collective-permute-done.38.refs_9_), channel_id=1, source_target_pairs={{0,8},{2,10},{4,12},{6,14},{8,16},{10,18},{12,20},{14,22},{16,24},... | collective-permute-start | bytes 786440 | tf_op jit(solution)/shard_map/ppermute | solution.py:509
  71.1 16.4 %collective-permute-start.4 = (bf16[256,1152]{1,0:T(8,128)(2,1)S(1)}, bf16[256,1152]{1,0:T(8,128)(2,1)S(1)}, u32[]{:S(2)}, u32[]{:S(2)}) collective-permute-start(bf16[256,1152]{1,0:T(8,128)(2,1)S(1)} %fusion.20.refs_0_.refs_8_), channel_id=1, source_target_pairs={{0,1},{1,0},{2,3},{3,2},{4,5},{5,4},{6,7},{7,6},{8,9},{9,8},{10,11... | collective-permute-start | bytes 1769480 | tf_op jit(solution)/shard_map/ppermute | solution.py:512
  84.8 19.5 %collective-permute-start.7 = (bf16[256,1152]{1,0:T(8,128)(2,1)S(1)}, bf16[256,1152]{1,0:T(8,128)(2,1)S(1)}, u32[]{:S(2)}, u32[]{:S(2)}) collective-permute-start(bf16[256,1152]{1,0:T(8,128)(2,1)S(1)} %collective-permute-done.3.refs_3_.refs_11_), channel_id=1, source_target_pairs={{0,1},{1,0},{2,3},{3,2},{4,5},{5,4},{6,7},{7,6},{8,9},{9,8},{10,11... | collective-permute-start | bytes 1769480 | tf_op jit(solution)/shard_map/ppermute | solution.py:512
  84.9 19.7 %collective-permute-start.6 = (bf16[256,1152]{1,0:T(8,128)(2,1)S(1)}, bf16[256,1152]{1,0:T(8,128)(2,1)S(1)}, u32[]{:S(2)}, u32[]{:S(2)}) collective-permute-start(bf16[256,1152]{1,0:T(8,128)(2,1)S(1)} %collective-permute-done.2.refs_2_.refs_10_), channel_id=1, source_target_pairs={{0,1},{1,0},{2,3},{3,2},{4,5},{5,4},{6,7},{7,6},{8,9},{9,8},{10,11... | collective-permute-start | bytes 1769480 | tf_op jit(solution)/shard_map/ppermute | solution.py:512
  85.4 19.2 %collective-permute-start.5 = (bf16[256,1152]{1,0:T(8,128)(2,1)S(1)}, bf16[256,1152]{1,0:T(8,128)(2,1)S(1)}, u32[]{:S(2)}, u32[]{:S(2)}) collective-permute-start(bf16[256,1152]{1,0:T(8,128)(2,1)S(1)} %collective-permute-done.1.refs_1_.refs_9_), channel_id=1, source_target_pairs={{0,1},{1,0},{2,3},{3,2},{4,5},{5,4},{6,7},{7,6},{8,9},{9,8},{10,11... | collective-permute-start | bytes 1769480 | tf_op jit(solution)/shard_map/ppermute | solution.py:512
  87.4 11.2 %collective-permute-start.19 = (bf16[512,256]{1,0:T(8,128)(2,1)}, bf16[512,256]{1,0:T(8,128)(2,1)S(1)}, u32[]{:S(2)}, u32[]{:S(2)}) collective-permute-start(bf16[512,256]{1,0:T(8,128)(2,1)} %copy-done.16), channel_id=1, source_target_pairs={{0,8},{2,10},{4,12},{6,14},{8,16},{10,18},{12,20},{14,22},{16,24},... | collective-permute-start | bytes 786440 | tf_op jit(solution)/shard_map/ppermute | solution.py:509
  91.8 12.5 %collective-permute-start.13 = (bf16[512,256]{1,0:T(8,128)(2,1)}, bf16[512,256]{1,0:T(8,128)(2,1)S(1)}, u32[]{:S(2)}, u32[]{:S(2)}) collective-permute-start(bf16[512,256]{1,0:T(8,128)(2,1)} %copy-done.18), channel_id=1, source_target_pairs={{0,8},{2,10},{4,12},{6,14},{8,16},{10,18},{12,20},{14,22},{16,24},... | collective-permute-start | bytes 786440 | tf_op jit(solution)/shard_map/ppermute | solution.py:509
  98.7 37.8 %collective-permute-start.46 = (bf16[512,256]{1,0:T(8,128)(2,1)}, bf16[512,256]{1,0:T(8,128)(2,1)S(1)}, u32[]{:S(2)}, u32[]{:S(2)}) collective-permute-start(bf16[512,256]{1,0:T(8,128)(2,1)} %copy-done.10), channel_id=1, source_target_pairs={{0,8},{2,10},{4,12},{6,14},{8,16},{10,18},{12,20},{14,22},{16,24},... | collective-permute-start | bytes 786440 | tf_op jit(solution)/shard_map/ppermute | solution.py:509
  104.3 32.8 %collective-permute-start.40 = (bf16[512,256]{1,0:T(8,128)(2,1)}, bf16[512,256]{1,0:T(8,128)(2,1)S(1)}, u32[]{:S(2)}, u32[]{:S(2)}) collective-permute-start(bf16[512,256]{1,0:T(8,128)(2,1)} %collective-permute-done.39.refs_10_), channel_id=1, source_target_pairs={{0,8},{2,10},{4,12},{6,14},{8,16},{10,18},{12,20},{14,22},{16,24},... | collective-permute-start | bytes 786440 | tf_op jit(solution)/shard_map/ppermute | solution.py:509
  104.3 42.5 %collective-permute-start.32 = (bf16[512,256]{1,0:T(8,128)(2,1)S(1)}, bf16[512,256]{1,0:T(8,128)(2,1)S(1)}, u32[]{:S(2)}, u32[]{:S(2)}) collective-permute-start(bf16[512,256]{1,0:T(8,128)(2,1)S(1)} %pad_maximum_fusion.3), channel_id=1, source_target_pairs={{0,2},{2,0},{4,6},{6,4},{8,10},{10,8},{12,14},{14,12},{16,18},{18,... | collective-permute-start | bytes 786440 | tf_op jit(solution)/shard_map/ppermute | solution.py:504
  120.2 36.2 %collective-permute-start.33 = (bf16[512,256]{1,0:T(8,128)(2,1)S(1)}, bf16[512,256]{1,0:T(8,128)(2,1)S(1)}, u32[]{:S(2)}, u32[]{:S(2)}) collective-permute-start(bf16[512,256]{1,0:T(8,128)(2,1)S(1)} %pad_maximum_fusion.4), channel_id=1, source_target_pairs={{0,4},{2,6},{4,0},{6,2},{8,12},{10,14},{12,8},{14,10},{16,20},{18,... | collective-permute-start | bytes 786440 | tf_op jit(solution)/shard_map/ppermute | solution.py:504
  134.1 24.1 %collective-permute-start.34 = (bf16[512,256]{1,0:T(8,128)(2,1)S(1)}, bf16[512,256]{1,0:T(8,128)(2,1)S(1)}, u32[]{:S(2)}, u32[]{:S(2)}) collective-permute-start(bf16[512,256]{1,0:T(8,128)(2,1)S(1)} %pad_maximum_fusion.5), channel_id=1, source_target_pairs={{0,6},{2,4},{4,2},{6,0},{8,14},{10,12},{12,10},{14,8},{16,22},{18,... | collective-permute-start | bytes 786440 | tf_op jit(solution)/shard_map/ppermute | solution.py:504
  136.4 11.7 %collective-permute-start.25 = (f32[8,1024]{1,0:T(8,128)S(1)}, f32[8,1024]{1,0:T(8,128)S(1)}, u32[]{:S(2)}, u32[]{:S(2)}) collective-permute-start(f32[8,1024]{1,0:T(8,128)S(1)} %add.236.refs_0_), channel_id=1, source_target_pairs={{0,6},{2,4},{4,2},{6,0},{8,14},{10,12},{12,10},{14,8},{16,22},{18,... | collective-permute-start | bytes 98312 | tf_op jit(solution)/shard_map/ppermute | solution.py:504
  144.3 15.0 %collective-permute-start.47 = (bf16[272,256]{1,0:T(8,128)(2,1)S(1)}, bf16[272,256]{1,0:T(8,128)(2,1)S(1)}, u32[]{:S(2)}, u32[]{:S(2)}) collective-permute-start(bf16[272,256]{1,0:T(8,128)(2,1)S(1)} %get-tuple-element.42), channel_id=1, source_target_pairs={{0,8},{2,10},{4,12},{6,14},{8,16},{10,18},{12,20},{14,22},{16,24},... | collective-permute-start | bytes 417800 | tf_op jit(solution)/shard_map/ppermute | solution.py:509
  150.7 15.8 %collective-permute-start.48 = (bf16[272,256]{1,0:T(8,128)(2,1)S(1)}, bf16[272,256]{1,0:T(8,128)(2,1)S(1)}, u32[]{:S(2)}, u32[]{:S(2)}) collective-permute-start(bf16[272,256]{1,0:T(8,128)(2,1)S(1)} %get-tuple-element.43), channel_id=1, source_target_pairs={{0,16},{2,18},{4,20},{6,22},{8,24},{10,26},{12,28},{14,30},{16,0},... | collective-permute-start | bytes 417800 | tf_op jit(solution)/shard_map/ppermute | solution.py:509
  152.3 14.3 %collective-permute-start.49 = (bf16[272,256]{1,0:T(8,128)(2,1)S(1)}, bf16[272,256]{1,0:T(8,128)(2,1)S(1)}, u32[]{:S(2)}, u32[]{:S(2)}) collective-permute-start(bf16[272,256]{1,0:T(8,128)(2,1)S(1)} %get-tuple-element.44), channel_id=1, source_target_pairs={{0,24},{2,26},{4,28},{6,30},{8,0},{10,2},{12,4},{14,6},{16,8},{18,... | collective-permute-start | bytes 417800 | tf_op jit(solution)/shard_map/ppermute | solution.py:509
  156.3 20.2 %collective-permute-start.26 = (bf16[256,256]{1,0:T(8,128)(2,1)S(1)}, bf16[256,256]{1,0:T(8,128)(2,1)S(1)}, u32[]{:S(2)}, u32[]{:S(2)}) collective-permute-start(bf16[256,256]{1,0:T(8,128)(2,1)S(1)} %get-tuple-element.33), channel_id=1, source_target_pairs={{0,2},{2,0},{4,6},{6,4},{8,10},{10,8},{12,14},{14,12},{16,18},{18,... | collective-permute-start | bytes 393224 | tf_op jit(solution)/shard_map/ppermute | solution.py:504
  158.2 19.0 %collective-permute-start.27 = (bf16[256,256]{1,0:T(8,128)(2,1)S(1)}, bf16[256,256]{1,0:T(8,128)(2,1)S(1)}, u32[]{:S(2)}, u32[]{:S(2)}) collective-permute-start(bf16[256,256]{1,0:T(8,128)(2,1)S(1)} %get-tuple-element.34), channel_id=1, source_target_pairs={{0,4},{2,6},{4,0},{6,2},{8,12},{10,14},{12,8},{14,10},{16,20},{18,... | collective-permute-start | bytes 393224 | tf_op jit(solution)/shard_map/ppermute | solution.py:504
  159.3 17.9 %collective-permute-start.28 = (bf16[256,256]{1,0:T(8,128)(2,1)S(1)}, bf16[256,256]{1,0:T(8,128)(2,1)S(1)}, u32[]{:S(2)}, u32[]{:S(2)}) collective-permute-start(bf16[256,256]{1,0:T(8,128)(2,1)S(1)} %get-tuple-element.35), channel_id=1, source_target_pairs={{0,6},{2,4},{4,2},{6,0},{8,14},{10,12},{12,10},{14,8},{16,22},{18,... | collective-permute-start | bytes 393224 | tf_op jit(solution)/shard_map/ppermute | solution.py:504
  (60 other events, 656.2 us)
